TPU v7x, 32 devices: a whole 2x2x4 slice. The times are simulated.
32 devices in a mesh: sp: 16 (over z, y, x), tp: 2 (over core).
Axes of the slice: x: 2, y: 2, z: 4, core: 2. Of those that a mesh axis runs over, the one named last changes fastest.
Arguments:
- stream: bfloat16 [4096, 2048], P('sp', 'tp'), may hold values from -6 to 6
- out_grad: bfloat16 [4096, 2048], P('sp', 'tp'), may hold values from -6 to 6
- gate_in: bfloat16 [4096, 1024], P('sp', 'tp'), may hold values from -6 to 6
- conv_gate: bfloat16 [4096, 1024], P('sp', 'tp'), may hold values from -6 to 6
- conv_value: bfloat16 [4096, 1024], P('sp', 'tp'), may hold values from -6 to 6
- taps: float32 [3, 1024], P(None, 'tp'), may hold values from -3.5 to 3.5
- w_out: bfloat16 [2048, 1024], P(None, 'tp'), may hold values from -0.1875 to 0.1875
- route_ids: int32 [4096, 2], P('sp'), may hold values from 0 to 15, all different within a row; in each aligned block of 256 rows (0 to 255, 256 to 511, ...) at most 64 rows name the same one
- route_weights: float32 [4096, 2], P('sp'), may hold values from 0.1 to 1
- w_gate: bfloat16 [16, 2048, 1024], P('sp', None, 'tp'), may hold values from -0.125 to 0.125
- w_up: bfloat16 [16, 2048, 1024], P('sp', None, 'tp'), may hold values from -0.125 to 0.125
- w_down: bfloat16 [16, 1024, 2048], P('sp', 'tp'), may hold values from -0.1875 to 0.1875
Outputs:
- stream_grad: bfloat16 [4096, 2048], P('sp', 'tp')
- gate_in_grad: bfloat16 [4096, 1024], P('sp', 'tp')
- conv_gate_grad: bfloat16 [4096, 1024], P('sp', 'tp')
- conv_value_grad: bfloat16 [4096, 1024], P('sp', 'tp')
- w_out_grad: float32 [2048, 1024], P('sp', 'tp')
- w_gate_grad: float32 [16, 2048, 1024], P('sp', None, 'tp')
- w_up_grad: float32 [16, 2048, 1024], P('sp', None, 'tp')
- w_down_grad: float32 [16, 1024, 2048], P('sp', 'tp')
Inputs may be any that keep to these rules, and one draw needn't show every extreme that they name: `route_ids`: the ids of one token differ. Within each aligned block of 256 tokens (the rows of one index of sp), no expert is named by more than 64 routes, and in every draw some expert is named by exactly 64 routes of some block.
All inputs are finite; a program needn't handle non-finite values.
Results may differ from a plain program's by a relative error of at most 0.009.
Values may be sent and summed in bfloat16 or wider, within the bound.
A program may use at most 128 MiB of HBM per device.

v0:
```python
import jax
import jax.numpy as jnp
from jax import lax
from jax.sharding import PartitionSpec as P


def passed_along(shard, axis, by):
    count = lax.axis_size(axis)
    pairs = [(i, i + by) for i in range(count) if 0 <= i + by < count]
    return lax.ppermute(shard, axis, pairs)


def expert_backward(sent_rows, sent_cot, w_gate, w_up, w_down):
    full_rows, full_cot = (
        lax.all_gather(sent_rows, "tp", axis=2, tiled=True),
        lax.all_gather(sent_cot, "tp", axis=2, tiled=True),
    )
    pre_gate = jnp.einsum("erd,edf->erf", full_rows, w_gate, preferred_element_type=jnp.float32)
    pre_up = jnp.einsum("erd,edf->erf", full_rows, w_up, preferred_element_type=jnp.float32)
    sigmoid_gate = jax.nn.sigmoid(pre_gate)
    silu_gate = pre_gate * sigmoid_gate
    hidden = (silu_gate * pre_up).astype(jnp.bfloat16)
    hidden_grad = jnp.einsum("erd,efd->erf", full_cot, w_down, preferred_element_type=jnp.float32)
    up_grad = (hidden_grad * silu_gate).astype(jnp.bfloat16)
    gate_grad = (
        hidden_grad * pre_up * sigmoid_gate * (1.0 + pre_gate * (1.0 - sigmoid_gate))
    ).astype(jnp.bfloat16)
    partial_terms = jnp.einsum(
        "erf,edf->erd", gate_grad, w_gate, preferred_element_type=jnp.float32
    )
    partial_terms = partial_terms + jnp.einsum(
        "erf,edf->erd", up_grad, w_up, preferred_element_type=jnp.float32
    )
    summed = lax.psum_scatter(
        partial_terms.astype(jnp.bfloat16), "tp", scatter_dimension=2, tiled=True
    )
    return (summed, (full_rows, full_cot, hidden, gate_grad, up_grad))


def weight_grads(saved):
    full_rows, full_cot, hidden, gate_grad, up_grad = saved
    gate_w_grad = jnp.einsum(
        "erd,erf->edf", full_rows, gate_grad, preferred_element_type=jnp.float32
    )
    up_w_grad = jnp.einsum("erd,erf->edf", full_rows, up_grad, preferred_element_type=jnp.float32)
    down_w_grad = jnp.einsum("erf,erd->efd", hidden, full_cot, preferred_element_type=jnp.float32)
    return (gate_w_grad, up_w_grad, down_w_grad)


def shards(
    stream,
    out_grad,
    gate_in,
    conv_gate,
    conv_value,
    taps,
    w_out,
    route_ids,
    route_weights,
    w_gate,
    w_up,
    w_down,
):
    tok_rows, half_width = stream.shape
    top_count = route_ids.shape[1]
    local_experts = w_gate.shape[0]
    sp_count = lax.axis_size("sp")
    experts = local_experts * sp_count
    capacity = 4 * tok_rows // experts
    route_total = tok_rows * top_count
    route_flat = route_ids.reshape(route_total)
    one_hot = (route_flat[:, None] == jnp.arange(experts, dtype=jnp.int32)[None, :]).astype(
        jnp.int32
    )
    slot_pos = jnp.sum(jnp.cumsum(one_hot, axis=0) * one_hot, axis=1) - 1
    slot_of = route_flat * capacity + slot_pos
    table = jnp.full((experts * capacity,), route_total, jnp.int32)
    table = table.at[slot_of].set(jnp.arange(route_total, dtype=jnp.int32))
    token_of = jnp.where(table < route_total, table // top_count, tok_rows)
    padded_stream = jnp.concatenate([stream, jnp.zeros((1, half_width), jnp.bfloat16)], axis=0)
    scaled = (route_weights[:, :, None] * out_grad[:, None, :].astype(jnp.float32)).astype(
        jnp.bfloat16
    )
    padded_cot = jnp.concatenate(
        [scaled.reshape(route_total, half_width), jnp.zeros((1, half_width), jnp.bfloat16)], axis=0
    )
    send_rows = padded_stream[token_of].reshape(experts, capacity, half_width)
    send_cot = padded_cot[table].reshape(experts, capacity, half_width)
    early_grads = []
    pending = []
    got_rows, got_cot = (
        lax.all_to_all(send_rows, "sp", split_axis=0, concat_axis=1, tiled=True),
        lax.all_to_all(send_cot, "sp", split_axis=0, concat_axis=1, tiled=True),
    )
    returned, saved = expert_backward(got_rows, got_cot, w_gate, w_up, w_down)
    early_grads.append(weight_grads(saved))
    came_back = lax.all_to_all(returned, "sp", split_axis=1, concat_axis=0, tiled=True)
    flat_rows = came_back.reshape(experts * capacity, half_width)
    route_rows = flat_rows[slot_of].astype(jnp.float32).reshape(tok_rows, top_count, half_width)
    input_grad = jnp.sum(route_rows, axis=1)
    stream_half = (out_grad.astype(jnp.float32) + input_grad).astype(jnp.bfloat16)
    stream_whole = lax.all_gather(stream_half, "tp", axis=1, tiled=True)
    mixer_grad = jnp.dot(stream_whole, w_out, preferred_element_type=jnp.float32).astype(
        jnp.bfloat16
    )
    depth = taps.shape[0]
    channels = conv_gate.shape[1]
    prod_rows = conv_gate.astype(jnp.float32) * conv_value.astype(jnp.float32)
    left_rows = passed_along(prod_rows[tok_rows - depth + 1 :], "sp", 1)
    padded = jnp.concatenate([left_rows, prod_rows], axis=0)
    conv_sum = jnp.zeros((tok_rows, channels), jnp.float32)
    for tap_index in range(depth):
        conv_sum = conv_sum + taps[tap_index][None, :] * padded[tap_index : tap_index + tok_rows]
    mixer_out = (gate_in.astype(jnp.float32) * conv_sum).astype(jnp.bfloat16)
    out_proj_grad = lax.psum_scatter(
        lax.dot_general(
            stream_whole, mixer_out, (((0,), (0,)), ((), ())), preferred_element_type=jnp.float32
        ),
        "sp",
        scatter_dimension=0,
        tiled=True,
    )
    mixer_wide = mixer_grad.astype(jnp.float32)
    gate_in_grad = (mixer_wide * conv_sum).astype(jnp.bfloat16)
    conv_inner = mixer_wide * gate_in.astype(jnp.float32)
    right_rows = passed_along(conv_inner[: depth - 1], "sp", -1)
    padded_back = jnp.concatenate([conv_inner, right_rows], axis=0)
    prod_grad = jnp.zeros((tok_rows, channels), jnp.float32)
    for tap_index in range(depth):
        offset = depth - 1 - tap_index
        prod_grad = prod_grad + taps[tap_index][None, :] * padded_back[offset : offset + tok_rows]
    conv_gate_grad = (prod_grad * conv_value.astype(jnp.float32)).astype(jnp.bfloat16)
    conv_value_grad = (prod_grad * conv_gate.astype(jnp.float32)).astype(jnp.bfloat16)
    all_grads = early_grads + [weight_grads(saved_item) for saved_item in pending]
    gate_w_grad, up_w_grad, down_w_grad = all_grads[0]
    return (
        stream_half,
        gate_in_grad,
        conv_gate_grad,
        conv_value_grad,
        out_proj_grad,
        gate_w_grad,
        up_w_grad,
        down_w_grad,
    )


def solution(mesh):
    placed = (
        P("sp", "tp"),
        P("sp", "tp"),
        P("sp", "tp"),
        P("sp", "tp"),
        P("sp", "tp"),
        P(None, "tp"),
        P(None, "tp"),
        P("sp", None),
        P("sp", None),
        P("sp", None, "tp"),
        P("sp", None, "tp"),
        P("sp", "tp", None),
    )
    return jax.shard_map(
        shards,
        mesh=mesh,
        in_specs=placed,
        out_specs=(
            P("sp", "tp"),
            P("sp", "tp"),
            P("sp", "tp"),
            P("sp", "tp"),
            P("sp", "tp"),
            P("sp", None, "tp"),
            P("sp", None, "tp"),
            P("sp", "tp", None),
        ),
        check_vma=False,
    )
```

profile of v0, /device:TPU:0, one launch (start us, length us, event | category | flops | bytes accessed | tf_op | source)
XLA Modules:
  0.0 390.6 jit_solution(3517894700962788309)
XLA Ops:
  14.5 5.3 %gather_fusion.1 = bf16[1024,1024]{1,0:T(8,128)(2,1)} fusion(bf16[257,1024]{1,0:T(8,128)(2,1)S(1)} %concatenate.13, s32[1024]{0:T(1024)S(1)} %get-tuple-element.19), kind=kCustom, calls=%fused_computation.1 | custom fusion | bytes 4198400 | tf_op jit(solution)/shard_map/gather | solution.py:87
  19.9 8.5 %all-to-all-start.1 = ((bf16[16,64,1024]{2,1,0:T(8,128)(2,1)}), bf16[16,64,1024]{2,1,0:T(8,128)(2,1)}, u32[]{:S(2)}, u32[]{:S(2)}) async-start(bf16[16,64,1024]{2,1,0:T(8,128)(2,1)} %bitcast.87), calls=%async_computation.1 | async-start | bytes 4194304 | tf_op jit(solution)/shard_map/all_to_all | solution.py:92
  30.6 3.6 mul.134
  34.3 37.2 %all-to-all-done.1 = bf16[16,64,1024]{2,1,0:T(8,128)(2,1)} async-done(((bf16[16,64,1024]{2,1,0:T(8,128)(2,1)}), bf16[16,64,1024]{2,1,0:T(8,128)(2,1)}, u32[]{:S(2)}, u32[]{:S(2)}) %all-to-all-start.1) | async-done | bytes 2097184 | tf_op jit(solution)/shard_map/all_to_all | solution.py:92
  73.4 5.3 %gather_fusion = bf16[1024,1024]{1,0:T(8,128)(2,1)} fusion(bf16[513,1024]{1,0:T(8,128)(2,1)S(1)} %concatenate.12, s32[1024]{0:T(1024)S(1)} %get-tuple-element.18), kind=kCustom, calls=%fused_computation | custom fusion | bytes 4198400 | tf_op jit(solution)/shard_map/gather | solution.py:88
  78.8 58.3 %all_to_all.33 = bf16[16,64,1024]{2,1,0:T(8,128)(2,1)} all-to-all(bf16[16,64,1024]{2,1,0:T(8,128)(2,1)} %bitcast.88), channel_id=1, replica_groups=mesh['sp'=16,'tp'=2] {'sp'}, dimensions={0} | all-to-all | bytes 4194304 | tf_op jit(solution)/shard_map/all_to_all | solution.py:93
  137.4 6.0 %fusion.5 = f32[1024,512]{1,0:T(8,128)} fusion(bf16[1,1024,2048]{2,1,0:T(8,128)(2,1)} %all-gather.6.cloned.1.call-done, bf16[1,2048,512]{2,1,0:T(8,128)(2,1)S(1)} %copy-done), kind=kOutput, calls=%fused_computation.10 | convolution fusion | flops 2147483648 | bytes 8388608 | tf_op jit(solution)/shard_map/erd,edf->erf/dot_general | solution.py:18
  143.4 3.7 fusion.7
  149.2 7.0 %multiply_convert_fusion.1 = (bf16[1024,512]{1,0:T(8,128)(2,1)S(1)}, bf16[1024,512]{1,0:T(8,128)(2,1)S(1)}) fusion(f32[1024,512]{1,0:T(8,128)} %fusion.5, f32[1024,512]{1,0:T(8,128)} %fusion.7, bf16[1,512,2048]{2,1,0:T(8,128)(2,1)} %param.23, bf16[1,1024,2048]{2,1,0:T(8,128)(2,1)} %all-gather.4.cloned.1.call-done), kind=kOutput, calls=%fused_computation.29 | convolution fusion | flops 2154299392 | bytes 12582912 | tf_op jit(solution)/shard_map/erd,efd->erf/dot_general | solution.py:23
  158.7 4.4 %fusion = bf16[1,1024,2048]{2,1,0:T(8,128)(2,1)} fusion(f32[1024,2048]{1,0:T(8,128)S(1)} %fusion.22, bf16[1024,512]{1,0:T(8,128)(2,1)S(1)} %get-tuple-element.12, bf16[1,2048,512]{2,1,0:T(8,128)(2,1)S(1)} %copy-done.14), kind=kOutput, calls=%fused_computation.5 | convolution fusion | flops 2151677952 | bytes 15728640 | tf_op jit(solution)/shard_map/erf,edf->erd/dot_general | solution.py:31
  163.1 13.2 %reduce-scatter.3.cloned.1.call-done = bf16[1,1024,1024]{2,1,0:T(8,128)(2,1)} async-done(((bf16[1,1024,2048]{2,1,0:T(8,128)(2,1)}), bf16[1,1024,1024]{2,1,0:T(8,128)(2,1)}) %reduce-scatter.3.cloned.1.call-update) | async-done | bytes 2097168 | tf_op jit(solution)/shard_map/reduce_scatter | solution.py:34
  176.3 7.1 %copy.43 = bf16[1,1024,1024]{2,0,1:T(2,128)(2,1)} copy(bf16[1,1024,1024]{2,1,0:T(8,128)(2,1)} %reduce-scatter.3.cloned.1.call-done) | data formatting | bytes 4194304 | tf_op jit(solution)/shard_map/reduce_scatter | solution.py:34
  183.9 12.8 %reduce.2 = bf16[1024,1024]{1,0:T(8,128)(2,1)S(1)} reduce(bf16[1024,1,1024]{2,1,0:T(2,128)(2,1)} %bitcast.85, bf16[]{:T(256)} %broadcast.124), dimensions={1}, to_apply=%bitcast.82.reduce_sub_computation | reduce | bytes 4194306
  199.4 6.9 %all-to-all-start.2 = ((bf16[16,2,32768]{2,1,0:T(2,128)(2,1)}), bf16[16,2,32768]{2,1,0:T(2,128)(2,1)S(1)}, u32[]{:S(2)}, u32[]{:S(2)}) async-start(bf16[16,2,32768]{2,1,0:T(2,128)(2,1)} %reshape.201), calls=%async_computation.3 | async-start | bytes 4194304 | tf_op jit(solution)/shard_map/all_to_all | solution.py:97
  206.4 43.2 %all-to-all-done.2 = bf16[16,2,32768]{2,1,0:T(2,128)(2,1)S(1)} async-done(((bf16[16,2,32768]{2,1,0:T(2,128)(2,1)}), bf16[16,2,32768]{2,1,0:T(2,128)(2,1)S(1)}, u32[]{:S(2)}, u32[]{:S(2)}) %all-to-all-start.2) | async-done | bytes 2097184 | tf_op jit(solution)/shard_map/all_to_all | solution.py:97
  249.6 6.7 %reshape.202 = bf16[1024,1,1024]{2,1,0:T(2,128)(2,1)} reshape(bf16[16,2,32768]{2,1,0:T(2,128)(2,1)S(1)} %all-to-all-done.2) | data formatting | bytes 4194304
  256.3 3.0 copy.42
  267.5 3.5 collective-permute-start
  272.1 9.0 %all-gather.8.cloned.1.call-done = bf16[256,2048]{1,0:T(8,128)(2,1)} async-done(((bf16[256,1024]{1,0:T(8,128)(2,1)}), bf16[256,2048]{1,0:T(8,128)(2,1)}) %all-gather.8.cloned.1.call-update) | async-done | bytes 1048592 | tf_op jit(solution)/shard_map/all_gather | solution.py:102
  281.1 3.5 multiply_convert_fusion.5
  288.6 6.7 %fusion.19 = f32[1,2048,512]{2,1,0:T(8,128)} fusion(bf16[1024,512]{1,0:T(8,128)(2,1)S(1)} %copy-done.16, bf16[1,1024,2048]{2,1,0:T(8,128)(2,1)} %all-gather.6.cloned.1.call-done), kind=kOutput, calls=%fused_computation.20 | convolution fusion | flops 2147483648 | bytes 9437184 | tf_op jit(solution)/shard_map/erd,erf->edf/dot_general | solution.py:45
  295.3 4.6 %fusion.13 = f32[1,512,2048]{2,1,0:T(8,128)} fusion(bf16[1,1024,2048]{2,1,0:T(8,128)(2,1)S(1)} %copy-done.12, f32[1024,512]{1,0:T(8,128)S(1)} %copy-done.20, f32[1024,512]{1,0:T(8,128)S(1)} %copy-done.19), kind=kOutput, calls=%fused_computation.18 | convolution fusion | flops 2150629376 | bytes 12582912 | tf_op jit(solution)/shard_map/erf,erd->efd/dot_general | solution.py:46
  301.4 4.5 %fusion.16 = f32[1,2048,512]{2,1,0:T(8,128)} fusion(bf16[1024,512]{1,0:T(8,128)(2,1)S(1)} %copy-done.18, bf16[1,1024,2048]{2,1,0:T(8,128)(2,1)S(1)} %copy-done.11), kind=kOutput, calls=%fused_computation.19 | convolution fusion | flops 2147483648 | bytes 9437184 | tf_op jit(solution)/shard_map/erd,erf->edf/dot_general | solution.py:42
  307.5 76.5 %reduce-scatter.5.cloned.1.call-done = f32[128,512]{1,0:T(8,128)} async-done(((f32[2048,512]{1,0:T(8,128)}), f32[128,512]{1,0:T(8,128)}) %reduce-scatter.5.cloned.1.call-update) | async-done | bytes 262160 | tf_op jit(solution)/shard_map/reduce_scatter | solution.py:115
  (95 shorter events, 35.8 us)
Async XLA Ops:
  7.2 130.2 %copy-start = (bf16[1,2048,512]{2,1,0:T(8,128)(2,1)S(1)}, bf16[1,2048,512]{2,1,0:T(8,128)(2,1)}, u32[]{:S(2)}) copy-start(bf16[1,2048,512]{2,1,0:T(8,128)(2,1)} %param.21) | copy-start | bytes 6291460
  19.9 8.6 %copy-start.9 = (f32[256,2]{0,1:T(2,128)S(1)}, f32[256,2]{0,1:T(2,128)}, u32[]{:S(2)}) copy-start(f32[256,2]{0,1:T(2,128)} %param.20) | copy-start | bytes 6148
  19.9 8.9 %copy-start.3 = (bf16[256,1024]{1,0:T(8,128)(2,1)S(1)}, bf16[256,1024]{1,0:T(8,128)(2,1)}, u32[]{:S(2)}) copy-start(bf16[256,1024]{1,0:T(8,128)(2,1)} %param.13) | copy-start | bytes 1572868
  19.9 51.6 %all-to-all-start.1 = ((bf16[16,64,1024]{2,1,0:T(8,128)(2,1)}), bf16[16,64,1024]{2,1,0:T(8,128)(2,1)}, u32[]{:S(2)}, u32[]{:S(2)}) async-start(bf16[16,64,1024]{2,1,0:T(8,128)(2,1)} %bitcast.87), calls=%async_computation.1 | async-start | bytes 4194304 | tf_op jit(solution)/shard_map/all_to_all | solution.py:92
  28.4 108.9 %all-gather.6.cloned.1.call-start = ((), (), s32[]{:S(2)}) async-start(), calls=%async_computation.6 | async-start | bytes 6291456 | tf_op jit(solution)/shard_map/all_gather | solution.py:15
  71.5 77.7 %all-gather.4.cloned.1.call-start = ((), (), s32[]{:S(2)}) async-start(), calls=%async_computation.5 | async-start | bytes 6291456 | tf_op jit(solution)/shard_map/all_gather | solution.py:16
  137.1 39.2 %reduce-scatter.3.cloned.1.call-start = ((), (), s32[]{:S(2)}) async-start(), calls=%async_computation.7 | async-start | bytes 6291456 | tf_op jit(solution)/shard_map/reduce_scatter | solution.py:34
  137.4 6.0 %copy-start.10 = (bf16[1,1024,2048]{2,1,0:T(8,128)(2,1)S(1)}, bf16[1,1024,2048]{2,1,0:T(8,128)(2,1)}, u32[]{:S(2)}) copy-start(bf16[1,1024,2048]{2,1,0:T(8,128)(2,1)} %all-gather.6.cloned.1.call-done) | copy-start | bytes 12582916
  137.4 6.0 %copy-start.13 = (bf16[1,2048,512]{2,1,0:T(8,128)(2,1)S(1)}, bf16[1,2048,512]{2,1,0:T(8,128)(2,1)}, u32[]{:S(2)}) copy-start(bf16[1,2048,512]{2,1,0:T(8,128)(2,1)} %param.22) | copy-start | bytes 6291460
  199.4 50.2 %all-to-all-start.2 = ((bf16[16,2,32768]{2,1,0:T(2,128)(2,1)}), bf16[16,2,32768]{2,1,0:T(2,128)(2,1)S(1)}, u32[]{:S(2)}, u32[]{:S(2)}) async-start(bf16[16,2,32768]{2,1,0:T(2,128)(2,1)} %reshape.201), calls=%async_computation.3 | async-start | bytes 4194304 | tf_op jit(solution)/shard_map/all_to_all | solution.py:97
  206.4 74.7 %all-gather.8.cloned.1.call-start = ((), (), s32[]{:S(2)}) async-start(), calls=%async_computation.8 | async-start | bytes 1572864 | tf_op jit(solution)/shard_map/all_gather | solution.py:102
  265.3 5.8 %copy-start.8 = (f32[3,512]{1,0:T(4,128)S(1)}, f32[3,512]{1,0:T(4,128)}, u32[]{:S(2)}) copy-start(f32[3,512]{1,0:T(4,128)} %param.17) | copy-start | bytes 18436
  265.3 15.8 %copy-start.7 = (bf16[256,512]{1,0:T(8,128)(2,1)S(1)}, bf16[256,512]{1,0:T(8,128)(2,1)}, u32[]{:S(2)}) copy-start(bf16[256,512]{1,0:T(8,128)(2,1)} %param.14) | copy-start | bytes 786436
  267.4 116.7 %reduce-scatter.5.cloned.1.call-start = ((), (), s32[]{:S(2)}) async-start(), calls=%async_computation.9 | async-start | bytes 4456448 | tf_op jit(solution)/shard_map/reduce_scatter | solution.py:115
  267.5 4.6 %collective-permute-start = (f32[2,512]{1,0:T(2,128)S(1)}, f32[2,512]{1,0:T(2,128)S(1)}, u32[]{:S(2)}, u32[]{:S(2)}) collective-permute-start(f32[2,512]{1,0:T(2,128)S(1)} %slice.54), channel_id=1, source_target_pairs={{0,2},{2,4},{4,6},{6,8},{8,10},{10,12},{12,14},{14,16},{16,18},{18... | collective-permute-start | bytes 12296 | tf_op jit(solution)/shard_map/ppermute | solution.py:10
  281.1 3.5 copy-start.2
  288.5 6.7 %copy-start.12 = (bf16[1,1024,2048]{2,1,0:T(8,128)(2,1)S(1)}, bf16[1,1024,2048]{2,1,0:T(8,128)(2,1)}, u32[]{:S(2)}) copy-start(bf16[1,1024,2048]{2,1,0:T(8,128)(2,1)} %all-gather.4.cloned.1.call-done) | copy-start | bytes 12582916
  288.5 6.7 %copy-start.19 = (f32[1024,512]{1,0:T(8,128)S(1)}, f32[1024,512]{1,0:T(8,128)}, u32[]{:S(2)}) copy-start(f32[1024,512]{1,0:T(8,128)} %fusion.5) | copy-start | bytes 6291460
  288.6 6.7 %copy-start.20 = (f32[1024,512]{1,0:T(8,128)S(1)}, f32[1024,512]{1,0:T(8,128)}, u32[]{:S(2)}) copy-start(f32[1024,512]{1,0:T(8,128)} %fusion.7) | copy-start | bytes 6291460
  295.3 6.0 %copy-start.11 = (bf16[1,1024,2048]{2,1,0:T(8,128)(2,1)S(1)}, bf16[1,1024,2048]{2,1,0:T(8,128)(2,1)}, u32[]{:S(2)}) copy-start(bf16[1,1024,2048]{2,1,0:T(8,128)(2,1)} %all-gather.6.cloned.1.call-done) | copy-start | bytes 12582916
  295.3 6.0 %copy-start.18 = (bf16[1024,512]{1,0:T(8,128)(2,1)S(1)}, bf16[1024,512]{1,0:T(8,128)(2,1)}, u32[]{:S(2)}) copy-start(bf16[1024,512]{1,0:T(8,128)(2,1)} %copy-done.17) | copy-start | bytes 3145732
  299.9 6.8 %copy-start.6 = (bf16[256,512]{1,0:T(8,128)(2,1)S(1)}, bf16[256,512]{1,0:T(8,128)(2,1)}, u32[]{:S(2)}) copy-start(bf16[256,512]{1,0:T(8,128)(2,1)} %param.16) | copy-start | bytes 786436
  299.9 5.9 %collective-permute-start.1 = (f32[2,512]{1,0:T(2,128)S(1)}, f32[2,512]{1,0:T(2,128)S(1)}, u32[]{:S(2)}, u32[]{:S(2)}) collective-permute-start(f32[2,512]{1,0:T(2,128)S(1)} %slice.57), channel_id=1, source_target_pairs={{2,0},{4,2},{6,4},{8,6},{10,8},{12,10},{14,12},{16,14},{18,16},{20... | collective-permute-start | bytes 12296 | tf_op jit(solution)/shard_map/ppermute | solution.py:10
  301.4 82.7 %copy-start.1 = (bf16[1,2048,512]{2,1,0:T(8,128)(2,1)S(1)}, bf16[1,2048,512]{2,1,0:T(8,128)(2,1)}, u32[]{:S(2)}) copy-start(bf16[1,2048,512]{2,1,0:T(8,128)(2,1)} %param.21) | copy-start | bytes 6291460
  (6 other events, 12.8 us)
Sparse Core Ops, SparseCore 0:
  71.6 18.0 all-gather.5
  137.2 11.9 all-gather.3
  163.2 13.0 reduce-scatter.2
  267.5 13.5 all-gather.7
  287.5 96.5 reduce-scatter.4
where the time goes:
time: 391 us
  waiting for transfers between devices  182 us (47%)
  blocking collectives  58.3 us (15%)
  local copies, waits for them, and re-layouts  46.4 us (12%)
  matrix products  45.5 us (12%)
  other arithmetic  23 us (6%)
  starting transfers between devices  20.8 us (5%)
  between operations  14.2 us (4%)
    reduce_scatter x1, waiting for transfers between devices, shards(): lax.psum_scatter(lax.dot_general(stream_whole, mixer_out, (((0,), (0,)),...  76.5 us
    all_to_all x1, blocking collectives, shards(): lax.all_to_all(send_cot, 'sp', split_axis=0, concat_axis=1, tiled=True)  58.3 us
    all_to_all x1, waiting for transfers between devices, shards(): lax.all_to_all(returned, 'sp', split_axis=1, concat_axis=0, tiled=True)  43.2 us
    all_to_all x1, waiting for transfers between devices, shards(): lax.all_to_all(send_rows, 'sp', split_axis=0, concat_axis=1, tiled=True)  37.2 us
    unnamed x48, local copies, waits for them, and re-layouts  15.2 us
    reduce_scatter x1, waiting for transfers between devices, expert_backward(): lax.psum_scatter(partial_terms.astype(jnp.bfloat16), 'tp', scatter_dimens...  13.2 us
    unnamed x1, other arithmetic  12.8 us
    all_gather x1, waiting for transfers between devices, shards(): stream_whole = lax.all_gather(stream_half, 'tp', axis=1, tiled=True)  8.98 us
  transfers between devices with their start and end apart: 9, of which 7 were waited for; matrix products, arithmetic and copies ran while one was open for 10% of the time, Pallas kernels for 0%

commit v1 on v0

v1 whole, which is shorter than its diff:
```python
import functools

import jax
import jax.numpy as jnp
from jax import lax
from jax.experimental import pallas as pl
from jax.experimental.pallas import tpu as pltpu
from jax.sharding import PartitionSpec as P

MESH = pl.DeviceIdType.MESH
GROUPS = 4
F32 = jnp.float32
BF16 = jnp.bfloat16


def passed_along(shard, axis, by):
    count = lax.axis_size(axis)
    pairs = [(i, i + by) for i in range(count) if 0 <= i + by < count]
    return lax.ppermute(shard, axis, pairs)


def dot(a, b, ca, cb):
    return lax.dot_general(a, b, (((ca,), (cb,)), ((), ())), preferred_element_type=F32)


def expert_kernel(
    count,
    cap,
    send_rows,
    send_cot,
    wg_hbm,
    wu_hbm,
    wd_hbm,
    back_out,
    gate_out,
    up_out,
    down_out,
    rows,
    cot,
    wg,
    wu,
    wd,
    pre_g,
    pre_u,
    hidden,
    gg,
    ug,
    part_out,
    part_in,
    ret,
    back,
    gate_f,
    up_f,
    down_f,
    w_sem,
    out_sem,
    send_sem,
    recv_sem,
    fsend_sem,
    frecv_sem,
    psend_sem,
    precv_sem,
    rsend_sem,
    rrecv_sem,
):
    me = lax.axis_index("sp")
    half = lax.axis_index("tp")
    other = 1 - half
    per = count // GROUPS
    height = per * cap
    width = rows.shape[2]
    tall = cap * count

    loads = []
    for n, (a, b) in enumerate(((wg_hbm, wg), (wu_hbm, wu), (wd_hbm, wd))):
        load = pltpu.make_async_copy(a.at[0], b, w_sem.at[n])
        load.start()
        loads.append(load)

    barrier = pltpu.get_barrier_semaphore()

    @pl.loop(1, count)
    def _(k):
        pl.semaphore_signal(
            barrier, inc=1, device_id=(lax.rem(me + k, count), half), device_id_type=MESH
        )

    pl.semaphore_signal(barrier, inc=1, device_id=(me, other), device_id_type=MESH)
    pl.semaphore_wait(barrier, count)

    def block(k):
        return pl.ds(pl.multiple_of(k * cap, cap), cap)

    def out_copy(which, src, dst, k):
        return pltpu.make_async_remote_copy(
            src_ref=src.at[block(k)],
            dst_ref=dst.at[half, block(k)],
            send_sem=send_sem.at[which, k],
            recv_sem=recv_sem.at[which, k],
            device_id=(lax.rem(me + k, count), half),
            device_id_type=MESH,
        )

    def pass_copy(which, src, k):
        return pltpu.make_async_remote_copy(
            src_ref=src,
            dst_ref=(rows if which == 0 else cot).at[half, block(k)],
            send_sem=fsend_sem.at[which, k],
            recv_sem=frecv_sem.at[which, k],
            device_id=(me, other),
            device_id_type=MESH,
        )

    def back_copy(k):
        return pltpu.make_async_remote_copy(
            src_ref=ret.at[block(k)],
            dst_ref=back.at[block(k)],
            send_sem=rsend_sem.at[k],
            recv_sem=rrecv_sem.at[k],
            device_id=(lax.rem(me - k + count, count), half),
            device_id_type=MESH,
        )

    def part_copy(g):
        at = pl.ds(pl.multiple_of(g * height, height), height)
        return pltpu.make_async_remote_copy(
            src_ref=part_out.at[at],
            dst_ref=part_in.at[at],
            send_sem=psend_sem.at[g],
            recv_sem=precv_sem.at[g],
            device_id=(me, other),
            device_id_type=MESH,
        )

    pairs = ((send_rows, rows), (send_cot, cot))
    for which, (src, dst) in enumerate(pairs):
        pass_copy(which, src.at[block(0)], 0).start()

        @pl.loop(1, count)
        def _(k):
            out_copy(which, src, dst, k).start()

    for which, (src, dst) in enumerate(pairs):
        dst[half, pl.ds(0, cap)] = src[pl.ds(0, cap)]
    for load in loads:
        load.wait()

    def gather_group(which, g):
        src, dst = pairs[which]

        @pl.loop(0, per)
        def _(j):
            k = g * per + j

            @pl.when(k > 0)
            def _():
                out_copy(which, src, dst, k).wait_recv()
                pass_copy(which, dst.at[half, block(k)], k).start()

        @pl.loop(0, per)
        def _(j):
            k = g * per + j
            pass_copy(which, dst.at[half, block(k)], k).wait_recv()

    @pl.loop(0, GROUPS)
    def _(g):
        gather_group(0, g)
        at = pl.ds(pl.multiple_of(g * height, height), height)
        left, right = rows[0, at], rows[1, at]
        pre_g[at] = dot(left, wg[:width], 1, 0) + dot(right, wg[width:], 1, 0)
        pre_u[at] = dot(left, wu[:width], 1, 0) + dot(right, wu[width:], 1, 0)

    mine_at = pl.ds(pl.multiple_of(half * width, width), width)
    other_at = pl.ds(pl.multiple_of(other * width, width), width)

    @pl.loop(0, GROUPS)
    def _(g):
        gather_group(1, g)
        at = pl.ds(pl.multiple_of(g * height, height), height)
        grad = dot(cot[0, at], wd[:, :width], 1, 1) + dot(cot[1, at], wd[:, width:], 1, 1)
        pg, pu = pre_g[at], pre_u[at]
        sig = jax.nn.sigmoid(pg)
        silu = pg * sig
        hidden[at] = (silu * pu).astype(BF16)
        ug_now = (grad * silu).astype(BF16)
        gg_now = (grad * pu * sig * (1.0 + pg * (1.0 - sig))).astype(BF16)
        ug[at] = ug_now
        gg[at] = gg_now
        far = dot(gg_now, wg[other_at], 1, 1) + dot(ug_now, wu[other_at], 1, 1)
        part_out[at] = far.astype(BF16)
        part_copy(g).start()
        near = dot(gg_now, wg[mine_at], 1, 1) + dot(ug_now, wu[mine_at], 1, 1)
        near = near.astype(BF16).astype(F32)
        part_copy(g).wait_recv()
        ret[at] = (near + part_in[at].astype(F32)).astype(BF16)

        @pl.loop(0, per)
        def _(j):
            k = g * per + j

            @pl.when(k > 0)
            def _():
                back_copy(k).start()

    back[pl.ds(0, cap)] = ret[pl.ds(0, cap)]

    tile = 256
    per_half = width // tile

    @pl.loop(0, 2 * per_half)
    def _(t):
        h, c = t // per_half, lax.rem(t, per_half)
        cols = pl.ds(pl.multiple_of(c * tile, tile), tile)
        to = pl.ds(pl.multiple_of(t * tile, tile), tile)
        x = rows[h, :, cols].T
        gate_f[to] = dot(x, gg[...], 1, 0)
        up_f[to] = dot(x, ug[...], 1, 0)

    stores = [
        pltpu.make_async_copy(gate_f, gate_out.at[0], out_sem.at[0]),
        pltpu.make_async_copy(up_f, up_out.at[0], out_sem.at[1]),
    ]
    for store in stores:
        store.start()

    hid_tile = min(256, hidden.shape[1])

    @pl.loop(0, hidden.shape[1] // hid_tile)
    def _(t):
        to = pl.ds(pl.multiple_of(t * hid_tile, hid_tile), hid_tile)
        x = hidden[:, to].T
        for h in range(2):
            down_f[to, h * width : (h + 1) * width] = dot(x, cot[h], 1, 0)

    stores.append(pltpu.make_async_copy(down_f, down_out.at[0], out_sem.at[2]))
    stores[-1].start()

    for which, (src, dst) in enumerate(pairs):

        @pl.loop(0, count)
        def _(k):
            @pl.when(k > 0)
            def _():
                out_copy(which, src, dst, k).wait_send()

            pass_copy(which, dst.at[half, block(k)], k).wait_send()

    @pl.loop(0, GROUPS)
    def _(g):
        part_copy(g).wait_send()

    @pl.loop(1, count)
    def _(k):
        back_copy(k).wait_send()
        back_copy(k).wait_recv()

    back_out[...] = back[...]
    for store in stores:
        store.wait()


def expert_pass(send_rows, send_cot, w_gate, w_up, w_down, cap):
    tall, width = send_rows.shape
    count = lax.axis_size("sp")
    deep, hid = w_gate.shape[1:]
    vmem = pl.BlockSpec(memory_space=pltpu.VMEM)
    anywhere = pl.BlockSpec(memory_space=pl.ANY)
    dma = pltpu.SemaphoreType.DMA
    return pl.pallas_call(
        functools.partial(expert_kernel, count, cap),
        out_shape=(
            jax.ShapeDtypeStruct((tall, width), BF16),
            jax.ShapeDtypeStruct((1, deep, hid), F32),
            jax.ShapeDtypeStruct((1, deep, hid), F32),
            jax.ShapeDtypeStruct((1, hid, deep), F32),
        ),
        in_specs=[vmem, vmem, anywhere, anywhere, anywhere],
        out_specs=(vmem, anywhere, anywhere, anywhere),
        scratch_shapes=[
            pltpu.VMEM((2, tall, width), BF16),
            pltpu.VMEM((2, tall, width), BF16),
            pltpu.VMEM((deep, hid), BF16),
            pltpu.VMEM((deep, hid), BF16),
            pltpu.VMEM((hid, deep), BF16),
            pltpu.VMEM((tall, hid), F32),
            pltpu.VMEM((tall, hid), F32),
            pltpu.VMEM((tall, hid), BF16),
            pltpu.VMEM((tall, hid), BF16),
            pltpu.VMEM((tall, hid), BF16),
            pltpu.VMEM((tall, width), BF16),
            pltpu.VMEM((tall, width), BF16),
            pltpu.VMEM((tall, width), BF16),
            pltpu.VMEM((tall, width), BF16),
            pltpu.VMEM((deep, hid), F32),
            pltpu.VMEM((deep, hid), F32),
            pltpu.VMEM((hid, deep), F32),
            dma((3,)),
            dma((3,)),
            dma((2, count)),
            dma((2, count)),
            dma((2, count)),
            dma((2, count)),
            dma((GROUPS,)),
            dma((GROUPS,)),
            dma((count,)),
            dma((count,)),
        ],
        compiler_params=pltpu.CompilerParams(
            collective_id=0, has_side_effects=True, vmem_limit_bytes=60 * 1024 * 1024
        ),
    )(send_rows, send_cot, w_gate, w_up, w_down)


def shards(
    stream,
    out_grad,
    gate_in,
    conv_gate,
    conv_value,
    taps,
    w_out,
    route_ids,
    route_weights,
    w_gate,
    w_up,
    w_down,
):
    tok_rows, half_width = stream.shape
    top_count = route_ids.shape[1]
    experts = w_gate.shape[0] * lax.axis_size("sp")
    capacity = 4 * tok_rows // experts
    route_total = tok_rows * top_count
    slots = experts * capacity
    me = lax.axis_index("sp")
    relative = lax.rem(route_ids - me + experts, experts)
    flat = relative.reshape(route_total)
    one_hot = flat[:, None] == jnp.arange(experts, dtype=jnp.int32)[None, :]
    order = jnp.arange(route_total, dtype=jnp.int32)
    earlier = (order[:, None] > order[None, :]).astype(BF16)
    ranks = dot(earlier, one_hot.astype(BF16), 1, 0)
    slot_pos = jnp.sum(jnp.where(one_hot, ranks, 0.0), axis=1).astype(jnp.int32)
    slot_of = (flat * capacity + slot_pos).reshape(tok_rows, top_count)
    places = jnp.arange(slots, dtype=jnp.int32)
    hits = [slot_of[:, k][None, :] == places[:, None] for k in range(top_count)]
    slot_weight = sum(
        jnp.sum(jnp.where(hits[k], route_weights[:, k][None, :], 0.0), axis=1)
        for k in range(top_count)
    )
    pick = functools.reduce(jnp.logical_or, hits).astype(BF16)
    send_rows = dot(pick, stream, 1, 0).astype(BF16)
    send_cot = (slot_weight[:, None] * dot(pick, out_grad, 1, 0)).astype(BF16)
    back, gate_w_grad, up_w_grad, down_w_grad = expert_pass(
        send_rows, send_cot, w_gate, w_up, w_down, capacity
    )
    input_grad = dot(pick, back, 0, 0)
    stream_half = (out_grad.astype(jnp.float32) + input_grad).astype(jnp.bfloat16)
    stream_whole = lax.all_gather(stream_half, "tp", axis=1, tiled=True)
    mixer_grad = jnp.dot(stream_whole, w_out, preferred_element_type=jnp.float32).astype(
        jnp.bfloat16
    )
    depth = taps.shape[0]
    channels = conv_gate.shape[1]
    prod_rows = conv_gate.astype(jnp.float32) * conv_value.astype(jnp.float32)
    left_rows = passed_along(prod_rows[tok_rows - depth + 1 :], "sp", 1)
    padded = jnp.concatenate([left_rows, prod_rows], axis=0)
    conv_sum = jnp.zeros((tok_rows, channels), jnp.float32)
    for tap_index in range(depth):
        conv_sum = conv_sum + taps[tap_index][None, :] * padded[tap_index : tap_index + tok_rows]
    mixer_out = (gate_in.astype(jnp.float32) * conv_sum).astype(jnp.bfloat16)
    out_proj_grad = lax.psum_scatter(
        dot(stream_whole, mixer_out, 0, 0).astype(BF16),
        "sp",
        scatter_dimension=0,
        tiled=True,
    ).astype(F32)
    mixer_wide = mixer_grad.astype(jnp.float32)
    gate_in_grad = (mixer_wide * conv_sum).astype(jnp.bfloat16)
    conv_inner = mixer_wide * gate_in.astype(jnp.float32)
    right_rows = passed_along(conv_inner[: depth - 1], "sp", -1)
    padded_back = jnp.concatenate([conv_inner, right_rows], axis=0)
    prod_grad = jnp.zeros((tok_rows, channels), jnp.float32)
    for tap_index in range(depth):
        offset = depth - 1 - tap_index
        prod_grad = prod_grad + taps[tap_index][None, :] * padded_back[offset : offset + tok_rows]
    conv_gate_grad = (prod_grad * conv_value.astype(jnp.float32)).astype(jnp.bfloat16)
    conv_value_grad = (prod_grad * conv_gate.astype(jnp.float32)).astype(jnp.bfloat16)
    return (
        stream_half,
        gate_in_grad,
        conv_gate_grad,
        conv_value_grad,
        out_proj_grad,
        gate_w_grad,
        up_w_grad,
        down_w_grad,
    )


def solution(mesh):
    placed = (
        P("sp", "tp"),
        P("sp", "tp"),
        P("sp", "tp"),
        P("sp", "tp"),
        P("sp", "tp"),
        P(None, "tp"),
        P(None, "tp"),
        P("sp", None),
        P("sp", None),
        P("sp", None, "tp"),
        P("sp", None, "tp"),
        P("sp", "tp", None),
    )
    return jax.shard_map(
        shards,
        mesh=mesh,
        in_specs=placed,
        out_specs=(
            P("sp", "tp"),
            P("sp", "tp"),
            P("sp", "tp"),
            P("sp", "tp"),
            P("sp", "tp"),
            P("sp", None, "tp"),
            P("sp", None, "tp"),
            P("sp", "tp", None),
        ),
        check_vma=False,
    )
```

time: 391 us -> 303 us (0.77)
  Pallas kernels: 0 us -> 171 us
  waiting for transfers between devices: 182 us -> 82.7 us
  blocking collectives: 58.3 us -> 0 us
  local copies, waits for them, and re-layouts: 46.4 us -> 12.6 us
  matrix products: 45.5 us -> 14.1 us
  starting transfers between devices: 20.8 us -> 2.65 us
  other arithmetic: 23 us -> 5.32 us
    pallas_call x0 -> x1, Pallas kernels: none -> 171 us  [expert_pass(): pl.pallas_call(functools.partial(expert_kernel, count, cap), out_shape=(j...]
    all_to_all x2 -> x0, waiting for transfers between devices: 80.4 us -> none  [the longest x1 43.2 us: shards(): lax.all_to_all(returned, 'sp', split_axis=1, concat_axis=0, tiled=True)]
    all_to_all x1 -> x0, blocking collectives: 58.3 us -> none  [shards(): lax.all_to_all(send_cot, 'sp', split_axis=0, concat_axis=1, tiled=True)]
    dot_general x9 -> x5, matrix products: 42 us -> 10.7 us  [dot(): lax.dot_general(a, b, (((ca,), (cb,)), ((), ())), preferred_element_type=...]
    all_to_all x2 -> x0, starting transfers between devices: 15.4 us -> none  [the longest x1 8.52 us: shards(): lax.all_to_all(send_rows, 'sp', split_axis=0, concat_axis=1, tiled=True)]
    reduce_scatter x2 -> x1, waiting for transfers between devices: 89.7 us -> 75.6 us  [shards(): lax.psum_scatter(dot(stream_whole, mixer_out, 0, 0).astype(BF16), 'sp', s...]
    unnamed x1 -> x0, other arithmetic: 12.8 us -> none
    gather x3 -> x0, local copies, waits for them, and re-layouts: 12.7 us -> none  [the longest x1 5.34 us: shards(): send_rows = padded_stream[token_of].reshape(experts, capacity, half_width)]
  transfers between devices with their start and end apart: 9 -> 4, of which waited for: 7 -> 4; matrix products, arithmetic and copies ran while one was open for 10% -> 1% of each run, Pallas kernels for 0% -> 0%
where the time goes in v1:
time: 303 us; the launch traced here: 302 us
  Pallas kernels  171 us (56%)
  waiting for transfers between devices  82.7 us (27%)
  between operations  14.2 us (5%)
  matrix products  14.1 us (5%)
  local copies, waits for them, and re-layouts  12.6 us (4%)
  other arithmetic  5.32 us (2%)
    pallas_call x1, Pallas kernels, expert_pass(): pl.pallas_call(functools.partial(expert_kernel, count, cap), out_shape=(j...  171 us
    reduce_scatter x1, waiting for transfers between devices, shards(): lax.psum_scatter(dot(stream_whole, mixer_out, 0, 0).astype(BF16), 'sp', s...  75.6 us
    unnamed x23, local copies, waits for them, and re-layouts  11.4 us
    dot_general x5, matrix products, dot(): lax.dot_general(a, b, (((ca,), (cb,)), ((), ())), preferred_element_type=...  10.7 us
  transfers between devices with their start and end apart: 4, of which 4 were waited for; matrix products, arithmetic and copies ran while one was open for 1% of the time, Pallas kernels for 0%

profile of v1, /device:TPU:0, one launch (start us, length us, event | category | flops | bytes accessed | tf_op | source)
XLA Modules:
  0.0 302.2 jit_solution(12263439243129818246)
XLA Ops:
  7.2 0.9 compare_select_fusion
  8.9 0.7 multiply_add_fusion
  9.6 0.8 fusion.32
  10.4 3.1 %convolution_convert_fusion.1.send_rows = bf16[1024,1024]{1,0:T(8,128)(2,1)} fusion(bf16[256,1024]{1,0:T(8,128)(2,1)} %param.12, s32[256]{0:T(256)S(1)} %bitcast.17, s32[256]{0:T(256)S(1)} %bitcast.13), kind=kOutput, calls=%fused_computation.2 | convolution fusion | flops 538705920 | bytes 2623488 | tf_op jit(solution)/shard_map/dot_general | solution.py:23
  13.5 0.3 select_reduce_fusion
  13.8 2.1 multiply_convert_fusion.send_cot
  15.9 170.6 %shard_map.179 = (bf16[1024,1024]{1,0:T(8,128)(2,1)}, f32[1,2048,512]{2,1,0:T(8,128)}, f32[1,2048,512]{2,1,0:T(8,128)}, f32[1,512,2048]{2,1,0:T(8,128)}) custom-call(bf16[1024,1024]{1,0:T(8,128)(2,1)} %convolution_convert_fusion.1.send_rows, bf16[1024,1024]{1,0:T(8,128)(2,1)} %multiply_convert_fusion.send_cot, bf16[1,2048,512]{2,1,0:T(8,128)(2,1)} %wg_hbm.1, ...), custom_call_target="tpu_custom_call" | custom-call | tf_op jit(solution)/shard_map/pallas_call | solution.py:269
  186.5 3.2 %fusion = bf16[256,1024]{1,0:T(8,128)(2,1)} fusion(bf16[1024,1024]{1,0:T(8,128)(2,1)} %get-tuple-element.12, bf16[256,1024]{1,0:T(8,128)(2,1)S(1)} %copy-done.9, s32[256]{0:T(256)S(1)} %bitcast.20, s32[256]{0:T(256)S(1)} %bitcast.16), kind=kOutput, calls=%fused_computation.4 | convolution fusion | flops 538443776 | bytes 3147776 | tf_op jit(solution)/shard_map/dot_general | solution.py:23
  189.9 0.8 copy-done.6
  190.7 1.3 collective-permute-start
  192.0 1.3 collective-permute-done
  193.3 1.5 all-gather.2.cloned.1.call-done
  194.8 3.4 %multiply_convert_fusion.1 = (bf16[256,512]{1,0:T(8,128)(2,1)}, f32[256,512]{1,0:T(8,128)S(1)}, f32[256,512]{1,0:T(8,128)S(1)}) fusion(f32[256,512]{1,0:T(8,128)} %copy-done.6, f32[512]{0:T(512)S(1)} %bitcast.23, f32[2,512]{1,0:T(2,128)S(1)} %collective-permute-done, f32[512]{0:T(512)S(1)} %bitcast.25, f32[512]{0:T(512)S(1)} %bitcast.21, ...), kind=kOutput, calls=%fused_computation.39 | convolution fusion | flops 538574848 | bytes 5253120 | tf_op jit(solution)/shard_map/dot_general | solution.py:358
  198.2 2.1 convolution_convert_fusion
  200.3 1.3 collective-permute-start.1
  201.6 4.2 %collective-permute-done.1 = f32[2,512]{1,0:T(2,128)S(1)} collective-permute-done((f32[2,512]{1,0:T(2,128)S(1)}, f32[2,512]{1,0:T(2,128)S(1)}, u32[]{:S(2)}, u32[]{:S(2)}) %collective-permute-start.1) | collective-permute-done | bytes 4128 | tf_op jit(solution)/shard_map/ppermute | solution.py:19
  205.8 0.9 fusion.15
  206.8 0.8 fusion.16
  207.5 75.6 %reduce-scatter.2.cloned.1.call-done = bf16[128,512]{1,0:T(8,128)(2,1)} async-done(((bf16[2048,512]{1,0:T(8,128)(2,1)}), bf16[128,512]{1,0:T(8,128)(2,1)}) %reduce-scatter.2.cloned.1.call-update) | async-done | bytes 131088 | tf_op jit(solution)/shard_map/reduce_scatter | solution.py:370
  283.2 1.6 convert_element_type.74
  284.8 4.8 %copy.46 = f32[1,2048,512]{2,1,0:T(8,128)} copy(f32[1,2048,512]{2,1,0:T(8,128)} %get-tuple-element.43) | data formatting | bytes 8388608
  289.6 2.1 copy.47
  291.8 1.6 copy-done.1
  293.3 2.0 copy.48
  (34 shorter events, 1.0 us)
Async XLA Ops:
  7.2 187.7 %copy-start = (bf16[2048,512]{1,0:T(8,128)(2,1)S(1)}, bf16[2048,512]{1,0:T(8,128)(2,1)}, u32[]{:S(2)}) copy-start(bf16[2048,512]{1,0:T(8,128)(2,1)} %param.18) | copy-start | bytes 6291460
  7.2 6.7 %copy-start.9 = (bf16[256,1024]{1,0:T(8,128)(2,1)S(1)}, bf16[256,1024]{1,0:T(8,128)(2,1)}, u32[]{:S(2)}) copy-start(bf16[256,1024]{1,0:T(8,128)(2,1)} %param.13) | copy-start | bytes 1572868
  7.2 187.6 %all-gather.2.cloned.1.call-start = ((), (), s32[]{:S(2)}) async-start(), calls=%async_computation.1 | async-start | bytes 1572864 | tf_op jit(solution)/shard_map/all_gather | solution.py:357
  186.5 3.3 %copy-start.4 = (bf16[256,512]{1,0:T(8,128)(2,1)S(1)}, bf16[256,512]{1,0:T(8,128)(2,1)}, u32[]{:S(2)}) copy-start(bf16[256,512]{1,0:T(8,128)(2,1)} %param.15) | copy-start | bytes 786436
  186.5 3.3 %copy-start.5 = (bf16[256,512]{1,0:T(8,128)(2,1)S(1)}, bf16[256,512]{1,0:T(8,128)(2,1)}, u32[]{:S(2)}) copy-start(bf16[256,512]{1,0:T(8,128)(2,1)} %param.16) | copy-start | bytes 786436
  186.5 5.5 %copy-start.8 = (f32[3,512]{1,0:T(4,128)S(1)}, f32[3,512]{1,0:T(4,128)}, u32[]{:S(2)}) copy-start(f32[3,512]{1,0:T(4,128)} %param.17) | copy-start | bytes 18436
  186.5 8.3 %copy-start.7 = (bf16[256,512]{1,0:T(8,128)(2,1)S(1)}, bf16[256,512]{1,0:T(8,128)(2,1)}, u32[]{:S(2)}) copy-start(bf16[256,512]{1,0:T(8,128)(2,1)} %param.14) | copy-start | bytes 786436
  189.8 93.4 %reduce-scatter.2.cloned.1.call-start = ((), (), s32[]{:S(2)}) async-start(), calls=%async_computation.2 | async-start | bytes 2228224 | tf_op jit(solution)/shard_map/reduce_scatter | solution.py:370
  189.9 0.8 copy-start.6
  190.7 2.6 collective-permute-start
  194.8 3.4 %copy-start.3 = (bf16[256,2048]{1,0:T(8,128)(2,1)S(1)}, bf16[256,2048]{1,0:T(8,128)(2,1)}, u32[]{:S(2)}) copy-start(bf16[256,2048]{1,0:T(8,128)(2,1)} %all-gather.2.cloned.1.call-done) | copy-start | bytes 3145732
  200.3 5.5 %collective-permute-start.1 = (f32[2,512]{1,0:T(2,128)S(1)}, f32[2,512]{1,0:T(2,128)S(1)}, u32[]{:S(2)}, u32[]{:S(2)}) collective-permute-start(f32[2,512]{1,0:T(2,128)S(1)} %slice.60), channel_id=1, source_target_pairs={{2,0},{4,2},{6,4},{8,6},{10,8},{12,10},{14,12},{16,14},{18,16},{20... | collective-permute-start | bytes 12296 | tf_op jit(solution)/shard_map/ppermute | solution.py:19
  284.8 4.8 %copy-start.2 = (f32[1,2048,512]{2,1,0:T(8,128)S(1)}, f32[1,2048,512]{2,1,0:T(8,128)}, u32[]{:S(2)}) copy-start(f32[1,2048,512]{2,1,0:T(8,128)} %get-tuple-element.44) | copy-start | bytes 12582916
  289.6 3.7 %copy-start.1 = (f32[1,512,2048]{2,1,0:T(8,128)S(1)}, f32[1,512,2048]{2,1,0:T(8,128)}, u32[]{:S(2)}) copy-start(f32[1,512,2048]{2,1,0:T(8,128)} %get-tuple-element.45) | copy-start | bytes 12582916
Sparse Core Ops, SparseCore 0:
  189.9 4.8 all-gather.1
  200.4 82.6 reduce-scatter.1

commit v2 on v1

--- a/solution.py
+++ b/solution.py
@@ -21,6 +21,13 @@
 
 def dot(a, b, ca, cb):
     return lax.dot_general(a, b, (((ca,), (cb,)), ((), ())), preferred_element_type=F32)
+
+
+def team_size(count):
+    size = 1
+    while size * size < count:
+        size *= 2
+    return size
 
 
 def expert_kernel(
@@ -31,7 +38,9 @@
     wg_hbm,
     wu_hbm,
     wd_hbm,
+    mix_in,
     back_out,
+    mix_out,
     gate_out,
     up_out,
     down_out,
@@ -52,6 +61,7 @@
     gate_f,
     up_f,
     down_f,
+    mix,
     w_sem,
     out_sem,
     send_sem,
@@ -62,6 +72,8 @@
     precv_sem,
     rsend_sem,
     rrecv_sem,
+    msend_sem,
+    mrecv_sem,
 ):
     me = lax.axis_index("sp")
     half = lax.axis_index("tp")
@@ -118,6 +130,20 @@
             send_sem=rsend_sem.at[k],
             recv_sem=rrecv_sem.at[k],
             device_id=(lax.rem(me - k + count, count), half),
+            device_id_type=MESH,
+        )
+
+    team = team_size(count)
+    place = lax.rem(me, team)
+    toks = mix_in.shape[0]
+
+    def mix_copy(j):
+        return pltpu.make_async_remote_copy(
+            src_ref=mix_in,
+            dst_ref=mix.at[pl.ds(pl.multiple_of(j * toks, toks), toks)],
+            send_sem=msend_sem.at[j],
+            recv_sem=mrecv_sem.at[j],
+            device_id=(me - place + lax.rem(place + j, team), half),
             device_id_type=MESH,
         )
 
@@ -140,6 +166,11 @@
         def _(k):
             out_copy(which, src, dst, k).start()
 
+    @pl.loop(1, team)
+    def _(j):
+        mix_copy(j).start()
+
+    mix[pl.ds(0, toks)] = mix_in[...]
     for which, (src, dst) in enumerate(pairs):
         dst[half, pl.ds(0, cap)] = src[pl.ds(0, cap)]
     for load in loads:
@@ -213,8 +244,8 @@
         cols = pl.ds(pl.multiple_of(c * tile, tile), tile)
         to = pl.ds(pl.multiple_of(t * tile, tile), tile)
         x = rows[h, :, cols].T
-        gate_f[to] = dot(x, gg[...], 1, 0)
-        up_f[to] = dot(x, ug[...], 1, 0)
+        gate_f[to] = dot(x, gg[...], 1, 0).astype(BF16)
+        up_f[to] = dot(x, ug[...], 1, 0).astype(BF16)
 
     stores = [
         pltpu.make_async_copy(gate_f, gate_out.at[0], out_sem.at[0]),
@@ -230,7 +261,7 @@
         to = pl.ds(pl.multiple_of(t * hid_tile, hid_tile), hid_tile)
         x = hidden[:, to].T
         for h in range(2):
-            down_f[to, h * width : (h + 1) * width] = dot(x, cot[h], 1, 0)
+            down_f[to, h * width : (h + 1) * width] = dot(x, cot[h], 1, 0).astype(BF16)
 
     stores.append(pltpu.make_async_copy(down_f, down_out.at[0], out_sem.at[2]))
     stores[-1].start()
@@ -254,15 +285,22 @@
         back_copy(k).wait_send()
         back_copy(k).wait_recv()
 
+    @pl.loop(1, team)
+    def _(j):
+        mix_copy(j).wait_send()
+        mix_copy(j).wait_recv()
+
+    mix_out[...] = mix[...]
     back_out[...] = back[...]
     for store in stores:
         store.wait()
 
 
-def expert_pass(send_rows, send_cot, w_gate, w_up, w_down, cap):
+def expert_pass(send_rows, send_cot, w_gate, w_up, w_down, mixer_out, cap):
     tall, width = send_rows.shape
     count = lax.axis_size("sp")
     deep, hid = w_gate.shape[1:]
+    team = team_size(count)
     vmem = pl.BlockSpec(memory_space=pltpu.VMEM)
     anywhere = pl.BlockSpec(memory_space=pl.ANY)
     dma = pltpu.SemaphoreType.DMA
@@ -270,12 +308,13 @@
         functools.partial(expert_kernel, count, cap),
         out_shape=(
             jax.ShapeDtypeStruct((tall, width), BF16),
-            jax.ShapeDtypeStruct((1, deep, hid), F32),
-            jax.ShapeDtypeStruct((1, deep, hid), F32),
-            jax.ShapeDtypeStruct((1, hid, deep), F32),
+            jax.ShapeDtypeStruct((team * mixer_out.shape[0], mixer_out.shape[1]), BF16),
+            jax.ShapeDtypeStruct((1, deep, hid), BF16),
+            jax.ShapeDtypeStruct((1, deep, hid), BF16),
+            jax.ShapeDtypeStruct((1, hid, deep), BF16),
         ),
-        in_specs=[vmem, vmem, anywhere, anywhere, anywhere],
-        out_specs=(vmem, anywhere, anywhere, anywhere),
+        in_specs=[vmem, vmem, anywhere, anywhere, anywhere, vmem],
+        out_specs=(vmem, vmem, anywhere, anywhere, anywhere),
         scratch_shapes=[
             pltpu.VMEM((2, tall, width), BF16),
             pltpu.VMEM((2, tall, width), BF16),
@@ -291,9 +330,10 @@
             pltpu.VMEM((tall, width), BF16),
             pltpu.VMEM((tall, width), BF16),
             pltpu.VMEM((tall, width), BF16),
-            pltpu.VMEM((deep, hid), F32),
-            pltpu.VMEM((deep, hid), F32),
-            pltpu.VMEM((hid, deep), F32),
+            pltpu.VMEM((deep, hid), BF16),
+            pltpu.VMEM((deep, hid), BF16),
+            pltpu.VMEM((hid, deep), BF16),
+            pltpu.VMEM((team * mixer_out.shape[0], mixer_out.shape[1]), BF16),
             dma((3,)),
             dma((3,)),
             dma((2, count)),
@@ -304,11 +344,223 @@
             dma((GROUPS,)),
             dma((count,)),
             dma((count,)),
+            dma((team,)),
+            dma((team,)),
         ],
         compiler_params=pltpu.CompilerParams(
             collective_id=0, has_side_effects=True, vmem_limit_bytes=60 * 1024 * 1024
         ),
-    )(send_rows, send_cot, w_gate, w_up, w_down)
+    )(send_rows, send_cot, w_gate, w_up, w_down, mixer_out)
+
+
+def mixer_kernel(
+    count,
+    sh,
+    w_out_hbm,
+    mix,
+    gate_in,
+    wog_out,
+    mg_out,
+    halo_out,
+    far,
+    w_out,
+    sg,
+    p_send,
+    p_recv,
+    h_send,
+    h_recv,
+    w_sem,
+    whole_sem,
+    gsend_sem,
+    grecv_sem,
+    fsend_sem,
+    frecv_sem,
+    own_sem,
+    psend_sem,
+    precv_sem,
+    hsem,
+):
+    me = lax.axis_index("sp")
+    half = lax.axis_index("tp")
+    other = 1 - half
+    team = team_size(count)
+    layers = count // team
+    place, layer = lax.rem(me, team), me // team
+    toks, width = sh.shape
+    per = layers // 2
+    blk = width // (team * per)
+    load = pltpu.make_async_copy(w_out_hbm, w_out, w_sem)
+    load.start()
+
+    def member(j):
+        return me - place + lax.rem(place + j, team)
+
+    def floor(i):
+        return lax.rem(layer + i, layers) * team + place
+
+    after, before = lax.rem(me + 1, count), lax.rem(me + count - 1, count)
+    barrier = pltpu.get_barrier_semaphore()
+
+    def greet(device):
+        pl.semaphore_signal(barrier, inc=1, device_id=device, device_id_type=MESH)
+
+    for j in range(1, team):
+        greet((member(j), half))
+    for i in range(1, layers):
+        greet((floor(i), half))
+    greet((me, other))
+    greet((after, half))
+    greet((before, half))
+    pl.semaphore_wait(barrier, team - 1 + layers - 1 + 3)
+
+    def remote(src, dst, send, recv, device):
+        return pltpu.make_async_remote_copy(
+            src_ref=src,
+            dst_ref=dst,
+            send_sem=send,
+            recv_sem=recv,
+            device_id=device,
+            device_id_type=MESH,
+        )
+
+    def cols(j, m):
+        at = (lax.rem(place + j, team) + team * m) * blk
+        return pl.ds(pl.multiple_of(at, blk), blk)
+
+    def spot(h, m, size):
+        return pl.ds(pl.multiple_of((h * per + m) * blk, blk), size)
+
+    def stripe(j):
+        return pl.ds(j * toks, toks)
+
+    def piece(j, m):
+        return remote(
+            sh.at[:, cols(j, m)],
+            sg.at[stripe(j), spot(half, m, blk)],
+            gsend_sem.at[j, m],
+            grecv_sem.at[j, m],
+            (member(j), half),
+        )
+
+    def own_piece(m):
+        return remote(
+            sh.at[:, cols(0, m)],
+            sg.at[stripe(0), spot(half, m, blk)],
+            own_sem.at[0, m],
+            own_sem.at[1, m],
+            (me, other),
+        )
+
+    def handed(j):
+        ref = sg.at[stripe(j), spot(half, 0, per * blk)]
+        return remote(ref, ref, fsend_sem.at[j], frecv_sem.at[j], (me, other))
+
+    whole = remote(sh, far, whole_sem.at[0], whole_sem.at[1], (me, other))
+    whole.start()
+    for j in range(1, team):
+        for m in range(per):
+            piece(j, m).start()
+    for m in range(per):
+        own_piece(m).start()
+        sg[stripe(0), spot(half, m, blk)] = sh[:, cols(0, m)]
+
+    load.wait()
+    near_at = pl.ds(pl.multiple_of(half * width, width), width)
+    far_at = pl.ds(pl.multiple_of(other * width, width), width)
+    grad = dot(sh[...], w_out[near_at], 1, 0)
+    whole.wait_recv()
+    grad = (grad + dot(far[...], w_out[far_at], 1, 0)).astype(BF16)
+    mg_out[...] = grad
+    h_send[...] = grad[:8].astype(F32) * gate_in[:8].astype(F32)
+    halo = remote(h_send, h_recv, hsem.at[0], hsem.at[1], (before, half))
+    halo.start()
+    for j in range(1, team):
+        for m in range(per):
+            piece(j, m).wait_recv()
+        handed(j).start()
+    for m in range(per):
+        own_piece(m).wait_recv()
+    for j in range(1, team):
+        handed(j).wait_recv()
+
+    def share(i):
+        at = pl.ds(pl.multiple_of(lax.rem(layer + i, layers) * blk, blk), blk)
+        return dot(sg[:, at].T, mix[...], 1, 0)
+
+    def part(i):
+        return remote(
+            p_send.at[i], p_recv.at[i], psend_sem.at[i], precv_sem.at[i], (floor(i), half)
+        )
+
+    @pl.loop(1, layers)
+    def _(i):
+        p_send[i] = share(i).astype(BF16)
+        part(i).start()
+
+    wog_out[...] = share(0)
+    for m in range(per):
+        own_piece(m).wait_send()
+    whole.wait_send()
+    for j in range(1, team):
+        for m in range(per):
+            piece(j, m).wait_send()
+        handed(j).wait_send()
+    halo.wait_send()
+    halo.wait_recv()
+    halo_out[...] = h_recv[...]
+
+    @pl.loop(1, layers)
+    def _(i):
+        part(i).wait_recv()
+        wog_out[...] += p_recv[i].astype(F32)
+
+    @pl.loop(1, layers)
+    def _(i):
+        part(i).wait_send()
+
+
+def mixer_pass(stream_half, w_out, mix, gate_in):
+    count = lax.axis_size("sp")
+    team = team_size(count)
+    layers = count // team
+    per = layers // 2
+    toks, width = stream_half.shape
+    deep, chans = w_out.shape
+    blk = deep // count
+    vmem = pl.BlockSpec(memory_space=pltpu.VMEM)
+    dma = pltpu.SemaphoreType.DMA
+    return pl.pallas_call(
+        functools.partial(mixer_kernel, count),
+        out_shape=(
+            jax.ShapeDtypeStruct((blk, chans), F32),
+            jax.ShapeDtypeStruct((toks, chans), BF16),
+            jax.ShapeDtypeStruct((8, chans), F32),
+        ),
+        in_specs=[vmem, pl.BlockSpec(memory_space=pl.ANY), vmem, vmem],
+        out_specs=(vmem, vmem, vmem),
+        scratch_shapes=[
+            pltpu.VMEM((toks, width), BF16),
+            pltpu.VMEM((deep, chans), BF16),
+            pltpu.VMEM((team * toks, layers * blk), BF16),
+            pltpu.VMEM((layers, blk, chans), BF16),
+            pltpu.VMEM((layers, blk, chans), BF16),
+            pltpu.VMEM((8, chans), F32),
+            pltpu.VMEM((8, chans), F32),
+            dma,
+            dma((2,)),
+            dma((team, per)),
+            dma((team, per)),
+            dma((team,)),
+            dma((team,)),
+            dma((2, per)),
+            dma((layers,)),
+            dma((layers,)),
+            dma((2,)),
+        ],
+        compiler_params=pltpu.CompilerParams(
+            collective_id=1, has_side_effects=True, vmem_limit_bytes=32 * 1024 * 1024
+        ),
+    )(stream_half, w_out, mix, gate_in)
 
 
 def shards(
@@ -349,15 +601,6 @@
     pick = functools.reduce(jnp.logical_or, hits).astype(BF16)
     send_rows = dot(pick, stream, 1, 0).astype(BF16)
     send_cot = (slot_weight[:, None] * dot(pick, out_grad, 1, 0)).astype(BF16)
-    back, gate_w_grad, up_w_grad, down_w_grad = expert_pass(
-        send_rows, send_cot, w_gate, w_up, w_down, capacity
-    )
-    input_grad = dot(pick, back, 0, 0)
-    stream_half = (out_grad.astype(jnp.float32) + input_grad).astype(jnp.bfloat16)
-    stream_whole = lax.all_gather(stream_half, "tp", axis=1, tiled=True)
-    mixer_grad = jnp.dot(stream_whole, w_out, preferred_element_type=jnp.float32).astype(
-        jnp.bfloat16
-    )
     depth = taps.shape[0]
     channels = conv_gate.shape[1]
     prod_rows = conv_gate.astype(jnp.float32) * conv_value.astype(jnp.float32)
@@ -367,16 +610,25 @@
     for tap_index in range(depth):
         conv_sum = conv_sum + taps[tap_index][None, :] * padded[tap_index : tap_index + tok_rows]
     mixer_out = (gate_in.astype(jnp.float32) * conv_sum).astype(jnp.bfloat16)
-    out_proj_grad = lax.psum_scatter(
-        dot(stream_whole, mixer_out, 0, 0).astype(BF16),
-        "sp",
-        scatter_dimension=0,
-        tiled=True,
-    ).astype(F32)
+    back, mix, gate_w_grad, up_w_grad, down_w_grad = expert_pass(
+        send_rows, send_cot, w_gate, w_up, w_down, mixer_out, capacity
+    )
+    input_grad = dot(pick, back, 0, 0)
+    stream_half = (out_grad.astype(jnp.float32) + input_grad).astype(jnp.bfloat16)
+    if w_out.shape[0] // lax.axis_size("sp") % 128 == 0:
+        out_proj_grad, mixer_grad, halo = mixer_pass(stream_half, w_out, mix, gate_in)
+    else:
+        stream_whole = lax.all_gather(stream_half, "tp", axis=1, tiled=True)
+        mixer_grad = dot(stream_whole, w_out, 1, 0).astype(BF16)
+        out_proj_grad = lax.psum_scatter(
+            dot(stream_whole, mixer_out, 0, 0).astype(BF16), "sp", scatter_dimension=0, tiled=True
+        ).astype(F32)
+        first = mixer_grad[: depth - 1].astype(F32) * gate_in[: depth - 1].astype(F32)
+        halo = passed_along(first, "sp", -1)
     mixer_wide = mixer_grad.astype(jnp.float32)
     gate_in_grad = (mixer_wide * conv_sum).astype(jnp.bfloat16)
     conv_inner = mixer_wide * gate_in.astype(jnp.float32)
-    right_rows = passed_along(conv_inner[: depth - 1], "sp", -1)
+    right_rows = jnp.where(me == lax.axis_size("sp") - 1, 0.0, halo[: depth - 1])
     padded_back = jnp.concatenate([conv_inner, right_rows], axis=0)
     prod_grad = jnp.zeros((tok_rows, channels), jnp.float32)
     for tap_index in range(depth):
@@ -390,9 +642,9 @@
         conv_gate_grad,
         conv_value_grad,
         out_proj_grad,
-        gate_w_grad,
-        up_w_grad,
-        down_w_grad,
+        gate_w_grad.astype(F32),
+        up_w_grad.astype(F32),
+        down_w_grad.astype(F32),
     )
 
 

time: 303 us -> 219 us (0.72); the launches traced: 302 us -> 215 us
  waiting for transfers between devices: 82.7 us -> 0.01 us
  Pallas kernels: 171 us -> 186 us
  between operations: 14.2 us -> 0.85 us
  local copies, waits for them, and re-layouts: 12.6 us -> 2.04 us
  other arithmetic: 5.32 us -> 14.1 us
  matrix products: 14.1 us -> 6.87 us
    reduce_scatter x1 -> x0, waiting for transfers between devices: 75.6 us -> none  [shards(): lax.psum_scatter(dot(stream_whole, mixer_out, 0, 0).astype(BF16), 'sp', s...]
    pallas_call x0 -> x1, Pallas kernels: none -> 16.9 us  [mixer_pass(): pl.pallas_call(functools.partial(mixer_kernel, count), out_shape=(jax.Sha...]
    unnamed x23 -> x25, local copies, waits for them, and re-layouts: 11.4 us -> 0.76 us
    convert_element_type x1 -> x4, other arithmetic: 1.63 us -> 8.66 us  [the longest x1 2.61 us: shards(): up_w_grad.astype(F32)]
    ppermute x2 -> x1, waiting for transfers between devices: 5.49 us -> 0.01 us  [passed_along(): return lax.ppermute(shard, axis, pairs)]
    dot_general x5 -> x4, matrix products: 10.7 us -> 6.87 us  [dot(): lax.dot_general(a, b, (((ca,), (cb,)), ((), ())), preferred_element_type=...]
    dot_general x1 -> x0, matrix products: 3.41 us -> none  [shards(): jnp.dot(stream_whole, w_out, preferred_element_type=jnp.float32)]
  transfers between devices with their start and end apart: 4 -> 1, of which waited for: 4 -> 0; matrix products, arithmetic and copies ran while one was open for 1% -> 3% of each run, Pallas kernels for 0% -> 0%
where the time goes in v2:
time: 219 us; the launch traced here: 215 us
  Pallas kernels  186 us (85%)
  other arithmetic  14.1 us (6%)
  matrix products  6.87 us (3%)
  starting transfers between devices  4.87 us (2%)
    pallas_call x1, Pallas kernels, expert_pass(): pl.pallas_call(functools.partial(expert_kernel, count, cap), out_shape=(j...  169 us
    pallas_call x1, Pallas kernels, mixer_pass(): pl.pallas_call(functools.partial(mixer_kernel, count), out_shape=(jax.Sha...  16.9 us
    dot_general x4, matrix products, dot(): lax.dot_general(a, b, (((ca,), (cb,)), ((), ())), preferred_element_type=...  6.87 us
    ppermute x1, starting transfers between devices, passed_along(): return lax.ppermute(shard, axis, pairs)  4.87 us
  transfers between devices with their start and end apart: 1, of which 0 were waited for; matrix products, arithmetic and copies ran while one was open for 3% of the time, Pallas kernels for 0%

profile of v2, /device:TPU:0, one launch (start us, length us, event | category | flops | bytes accessed | tf_op | source)
XLA Modules:
  0.0 215.0 jit_solution(10819123189968342131)
XLA Ops:
  0.7 1.2 convert_multiply_fusion.3
  1.9 4.9 %collective-permute-start = (f32[2,512]{1,0:T(2,128)S(1)}, f32[2,512]{1,0:T(2,128)S(1)}, u32[]{:S(2)}, u32[]{:S(2)}) collective-permute-start(f32[2,512]{1,0:T(2,128)S(1)} %slice.57), channel_id=1, source_target_pairs={{0,2},{2,4},{4,6},{6,8},{8,10},{10,12},{12,14},{14,16},{16,18},{18... | collective-permute-start | bytes 12296 | tf_op jit(solution)/shard_map/ppermute | solution.py:19
  6.7 0.8 fusion.31
  7.5 0.7 compare_select_fusion
  8.2 0.1 copy.41
  8.3 0.1 eq.48
  8.5 0.3 fusion.1
  8.8 0.1 convert_element_type.60
  8.9 0.1 copy.42
  9.0 0.7 multiply_add_fusion
  9.7 2.0 convolution_convert_fusion.send_rows
  11.8 0.3 select_reduce_fusion
  12.1 2.1 multiply_convert_fusion.send_cot
  14.2 0.9 fusion.14
  15.1 169.4 %shard_map.179 = (bf16[1024,1024]{1,0:T(8,128)(2,1)}, bf16[1024,512]{1,0:T(8,128)(2,1)}, bf16[1,2048,512]{2,1,0:T(8,128)(2,1)}, bf16[1,2048,512]{2,1,0:T(8,128)(2,1)}, bf16[1,512,2048]{2,1,0:T(8,128)(2,1)}) custom-call(bf16[1024,1024]{1,0:T(8,128)(2,1)} %convolution_convert_fusion.send_rows, bf16[1024,1024]{1,0:T(8,128)(2,1)} %multiply_convert_fusion.send_cot, ...), custom_call_target="tpu_custom_call" | custom-call | tf_op jit(solution)/shard_map/pallas_call | solution.py:307
  184.5 2.5 %fusion.sh = bf16[256,1024]{1,0:T(8,128)(2,1)S(1)} fusion(bf16[1024,1024]{1,0:T(8,128)(2,1)} %get-tuple-element.16, bf16[256,1024]{1,0:T(8,128)(2,1)S(1)} %copy-done.11, s32[256]{0:T(256)S(1)} %bitcast.23, s32[256]{0:T(256)S(1)} %bitcast.19), kind=kOutput, calls=%fused_computation.3 | convolution fusion | flops 538443776 | bytes 3147776 | tf_op jit(solution)/shard_map/dot_general | solution.py:23
  187.1 16.9 %shard_map.180 = (f32[128,512]{1,0:T(8,128)S(1)}, bf16[256,512]{1,0:T(8,128)(2,1)S(1)}, f32[8,512]{1,0:T(8,128)S(1)}) custom-call(bf16[256,1024]{1,0:T(8,128)(2,1)S(1)} %fusion.sh, bf16[2048,512]{1,0:T(8,128)(2,1)S(1)} %copy-done.2, bf16[1024,512]{1,0:T(8,128)(2,1)S(1)} %copy-done.3, bf16[256,512]{1,0:T(8,128)(2,1)S(1)} %copy-done.1), custom_call_target="tpu_custom_call" | custom-call | tf_op jit(solution)/shard_map/pallas_call | solution.py:532
  204.0 0.8 convert_multiply_fusion
  204.9 0.9 fusion.15
  205.8 0.8 fusion.16
  206.5 2.6 %convert_element_type.72 = f32[1,2048,512]{2,1,0:T(8,128)} convert(bf16[1,2048,512]{2,1,0:T(8,128)(2,1)S(1)} %copy-done.7) | non-fusion elementwise | flops 1048576 | bytes 6291456 | tf_op jit(solution)/shard_map/convert_element_type | solution.py:645
  209.2 2.6 %convert_element_type.73 = f32[1,2048,512]{2,1,0:T(8,128)} convert(bf16[1,2048,512]{2,1,0:T(8,128)(2,1)S(1)} %copy-done.6) | non-fusion elementwise | flops 1048576 | bytes 6291456 | tf_op jit(solution)/shard_map/convert_element_type | solution.py:646
  211.8 2.5 %convert_element_type.74 = f32[1,512,2048]{2,1,0:T(8,128)} convert(bf16[1,512,2048]{2,1,0:T(8,128)(2,1)S(1)} %copy-done.5) | non-fusion elementwise | flops 1048576 | bytes 6291456 | tf_op jit(solution)/shard_map/convert_element_type | solution.py:647
  214.3 0.7 copy.44
  (31 shorter events, 0.1 us)
Async XLA Ops:
  0.6 9.1 %copy-start = (bf16[256,1024]{1,0:T(8,128)(2,1)S(1)}, bf16[256,1024]{1,0:T(8,128)(2,1)}, u32[]{:S(2)}) copy-start(bf16[256,1024]{1,0:T(8,128)(2,1)} %param.12) | copy-start | bytes 1572868
  0.6 11.5 %copy-start.11 = (bf16[256,1024]{1,0:T(8,128)(2,1)S(1)}, bf16[256,1024]{1,0:T(8,128)(2,1)}, u32[]{:S(2)}) copy-start(bf16[256,1024]{1,0:T(8,128)(2,1)} %param.13) | copy-start | bytes 1572868
  1.9 12.3 %collective-permute-start = (f32[2,512]{1,0:T(2,128)S(1)}, f32[2,512]{1,0:T(2,128)S(1)}, u32[]{:S(2)}, u32[]{:S(2)}) collective-permute-start(f32[2,512]{1,0:T(2,128)S(1)} %slice.57), channel_id=1, source_target_pairs={{0,2},{2,4},{4,6},{6,8},{8,10},{10,12},{12,14},{14,16},{16,18},{18... | collective-permute-start | bytes 12296 | tf_op jit(solution)/shard_map/ppermute | solution.py:19
  11.8 2.4 %copy-start.10 = (f32[3,512]{1,0:T(4,128)S(1)}, f32[3,512]{1,0:T(4,128)}, u32[]{:S(2)}) copy-start(f32[3,512]{1,0:T(4,128)} %param.17) | copy-start | bytes 18436
  11.8 2.5 %copy-start.1 = (bf16[256,512]{1,0:T(8,128)(2,1)S(1)}, bf16[256,512]{1,0:T(8,128)(2,1)}, u32[]{:S(2)}) copy-start(bf16[256,512]{1,0:T(8,128)(2,1)} %gate_in.1) | copy-start | bytes 786436
  184.5 2.5 %copy-start.2 = (bf16[2048,512]{1,0:T(8,128)(2,1)S(1)}, bf16[2048,512]{1,0:T(8,128)(2,1)}, u32[]{:S(2)}) copy-start(bf16[2048,512]{1,0:T(8,128)(2,1)} %w_out_hbm.1) | copy-start | bytes 6291460
  184.5 2.5 %copy-start.3 = (bf16[1024,512]{1,0:T(8,128)(2,1)S(1)}, bf16[1024,512]{1,0:T(8,128)(2,1)}, u32[]{:S(2)}) copy-start(bf16[1024,512]{1,0:T(8,128)(2,1)} %get-tuple-element.17.mix) | copy-start | bytes 3145732
  187.0 17.8 %copy-start.4 = (bf16[256,1024]{1,0:T(8,128)(2,1)}, bf16[256,1024]{1,0:T(8,128)(2,1)S(1)}, u32[]{:S(2)}) copy-start(bf16[256,1024]{1,0:T(8,128)(2,1)S(1)} %fusion.sh) | copy-start | bytes 1572868
  187.1 17.8 %copy-start.8 = (bf16[256,512]{1,0:T(8,128)(2,1)S(1)}, bf16[256,512]{1,0:T(8,128)(2,1)}, u32[]{:S(2)}) copy-start(bf16[256,512]{1,0:T(8,128)(2,1)} %param.15) | copy-start | bytes 786436
  204.0 1.8 copy-start.9
  204.0 2.5 %copy-start.7 = (bf16[1,2048,512]{2,1,0:T(8,128)(2,1)S(1)}, bf16[1,2048,512]{2,1,0:T(8,128)(2,1)}, u32[]{:S(2)}) copy-start(bf16[1,2048,512]{2,1,0:T(8,128)(2,1)} %get-tuple-element.21) | copy-start | bytes 6291460
  206.5 2.6 %copy-start.6 = (bf16[1,2048,512]{2,1,0:T(8,128)(2,1)S(1)}, bf16[1,2048,512]{2,1,0:T(8,128)(2,1)}, u32[]{:S(2)}) copy-start(bf16[1,2048,512]{2,1,0:T(8,128)(2,1)} %get-tuple-element.22) | copy-start | bytes 6291460
  209.2 2.6 %copy-start.5 = (bf16[1,512,2048]{2,1,0:T(8,128)(2,1)S(1)}, bf16[1,512,2048]{2,1,0:T(8,128)(2,1)}, u32[]{:S(2)}) copy-start(bf16[1,512,2048]{2,1,0:T(8,128)(2,1)} %get-tuple-element.23) | copy-start | bytes 6291460

commit v3 on v2

--- a/solution.py
+++ b/solution.py
@@ -39,7 +39,12 @@
     wu_hbm,
     wd_hbm,
     mix_in,
+    stream_in,
+    grad_in,
+    pick,
+    scale,
     back_out,
+    cross_out,
     mix_out,
     gate_out,
     up_out,
@@ -62,6 +67,13 @@
     up_f,
     down_f,
     mix,
+    toks_in,
+    rel_rows,
+    rel_cot,
+    cross_src,
+    cross_dst,
+    x_send,
+    x_recv,
     w_sem,
     out_sem,
     send_sem,
@@ -81,7 +93,10 @@
     per = count // GROUPS
     height = per * cap
     width = rows.shape[2]
-    tall = cap * count
+    ring = count // 2
+    loc = lax.rem(me, ring)
+    base = me - loc
+    mirror = (lax.rem(me + ring, count), half)
 
     loads = []
     for n, (a, b) in enumerate(((wg_hbm, wg), (wu_hbm, wu), (wd_hbm, wd))):
@@ -91,25 +106,26 @@
 
     barrier = pltpu.get_barrier_semaphore()
 
-    @pl.loop(1, count)
+    @pl.loop(1, ring)
     def _(k):
         pl.semaphore_signal(
-            barrier, inc=1, device_id=(lax.rem(me + k, count), half), device_id_type=MESH
+            barrier, inc=1, device_id=(base + lax.rem(loc + k, ring), half), device_id_type=MESH
         )
 
     pl.semaphore_signal(barrier, inc=1, device_id=(me, other), device_id_type=MESH)
-    pl.semaphore_wait(barrier, count)
+    pl.semaphore_signal(barrier, inc=1, device_id=mirror, device_id_type=MESH)
+    pl.semaphore_wait(barrier, ring + 1)
 
     def block(k):
         return pl.ds(pl.multiple_of(k * cap, cap), cap)
 
     def out_copy(which, src, dst, k):
         return pltpu.make_async_remote_copy(
-            src_ref=src.at[block(k)],
+            src_ref=src.at[block(lax.rem(k, ring))],
             dst_ref=dst.at[half, block(k)],
             send_sem=send_sem.at[which, k],
             recv_sem=recv_sem.at[which, k],
-            device_id=(lax.rem(me + k, count), half),
+            device_id=(base + lax.rem(loc + k, ring), half),
             device_id_type=MESH,
         )
 
@@ -129,7 +145,7 @@
             dst_ref=back.at[block(k)],
             send_sem=rsend_sem.at[k],
             recv_sem=rrecv_sem.at[k],
-            device_id=(lax.rem(me - k + count, count), half),
+            device_id=(base + lax.rem(loc - k + 2 * ring, ring), half),
             device_id_type=MESH,
         )
 
@@ -158,11 +174,28 @@
             device_id_type=MESH,
         )
 
+    def cross_copy(n, src, dst):
+        return pltpu.make_async_remote_copy(
+            src_ref=src,
+            dst_ref=dst,
+            send_sem=x_send.at[n],
+            recv_sem=x_recv.at[n],
+            device_id=mirror,
+            device_id_type=MESH,
+        )
+
+    crossing = (
+        cross_copy(0, stream_in, toks_in.at[0]),
+        cross_copy(1, grad_in, toks_in.at[1]),
+        cross_copy(2, cross_src, cross_dst),
+    )
+    crossing[0].start()
+    crossing[1].start()
     pairs = ((send_rows, rows), (send_cot, cot))
     for which, (src, dst) in enumerate(pairs):
         pass_copy(which, src.at[block(0)], 0).start()
 
-        @pl.loop(1, count)
+        @pl.loop(1, ring)
         def _(k):
             out_copy(which, src, dst, k).start()
 
@@ -173,6 +206,18 @@
     mix[pl.ds(0, toks)] = mix_in[...]
     for which, (src, dst) in enumerate(pairs):
         dst[half, pl.ds(0, cap)] = src[pl.ds(0, cap)]
+    for which, (rel, dst) in enumerate(((rel_rows, rows), (rel_cot, cot))):
+        crossing[which].wait_recv()
+        chosen = dot(pick[...], toks_in[which], 1, 0)
+        chosen = (chosen if which == 0 else scale[...] * chosen).astype(BF16)
+        rel[...] = chosen
+        dst[half, pl.ds(ring * cap, cap)] = chosen[:cap]
+        pass_copy(which, rel.at[block(0)], ring).start()
+
+        @pl.loop(ring + 1, count)
+        def _(k):
+            out_copy(which, rel, dst, k).start()
+
     for load in loads:
         load.wait()
 
@@ -183,7 +228,7 @@
         def _(j):
             k = g * per + j
 
-            @pl.when(k > 0)
+            @pl.when(lax.rem(k, ring) > 0)
             def _():
                 out_copy(which, src, dst, k).wait_recv()
                 pass_copy(which, dst.at[half, block(k)], k).start()
@@ -229,11 +274,12 @@
         def _(j):
             k = g * per + j
 
-            @pl.when(k > 0)
+            @pl.when(lax.rem(k, ring) > 0)
             def _():
                 back_copy(k).start()
 
     back[pl.ds(0, cap)] = ret[pl.ds(0, cap)]
+    back[pl.ds(ring * cap, cap)] = ret[pl.ds(ring * cap, cap)]
 
     tile = 256
     per_half = width // tile
@@ -266,11 +312,18 @@
     stores.append(pltpu.make_async_copy(down_f, down_out.at[0], out_sem.at[2]))
     stores[-1].start()
 
+    @pl.loop(ring + 1, count)
+    def _(k):
+        back_copy(k).wait_recv()
+
+    cross_src[...] = dot(pick[...], back[ring * cap :], 0, 0).astype(BF16)
+    crossing[2].start()
+
     for which, (src, dst) in enumerate(pairs):
 
         @pl.loop(0, count)
         def _(k):
-            @pl.when(k > 0)
+            @pl.when(lax.rem(k, ring) > 0)
             def _():
                 out_copy(which, src, dst, k).wait_send()
 
@@ -280,10 +333,14 @@
     def _(g):
         part_copy(g).wait_send()
 
-    @pl.loop(1, count)
+    @pl.loop(1, ring)
     def _(k):
         back_copy(k).wait_send()
         back_copy(k).wait_recv()
+
+    @pl.loop(ring + 1, count)
+    def _(k):
+        back_copy(k).wait_send()
 
     @pl.loop(1, team)
     def _(j):
@@ -291,13 +348,21 @@
         mix_copy(j).wait_recv()
 
     mix_out[...] = mix[...]
-    back_out[...] = back[...]
+    back_out[...] = back[: ring * cap]
+    for copy in crossing:
+        copy.wait_send()
+    crossing[2].wait_recv()
+    cross_out[...] = cross_dst[...]
     for store in stores:
         store.wait()
 
 
-def expert_pass(send_rows, send_cot, w_gate, w_up, w_down, mixer_out, cap):
-    tall, width = send_rows.shape
+def expert_pass(
+    send_rows, send_cot, w_gate, w_up, w_down, mixer_out, stream, out_grad, pick, scale, cap
+):
+    short, width = send_rows.shape
+    tall = 2 * short
+    toks = stream.shape[0]
     count = lax.axis_size("sp")
     deep, hid = w_gate.shape[1:]
     team = team_size(count)
@@ -307,14 +372,15 @@
     return pl.pallas_call(
         functools.partial(expert_kernel, count, cap),
         out_shape=(
-            jax.ShapeDtypeStruct((tall, width), BF16),
+            jax.ShapeDtypeStruct((short, width), BF16),
+            jax.ShapeDtypeStruct((toks, width), BF16),
             jax.ShapeDtypeStruct((team * mixer_out.shape[0], mixer_out.shape[1]), BF16),
             jax.ShapeDtypeStruct((1, deep, hid), BF16),
             jax.ShapeDtypeStruct((1, deep, hid), BF16),
             jax.ShapeDtypeStruct((1, hid, deep), BF16),
         ),
-        in_specs=[vmem, vmem, anywhere, anywhere, anywhere, vmem],
-        out_specs=(vmem, vmem, anywhere, anywhere, anywhere),
+        in_specs=[vmem, vmem, anywhere, anywhere, anywhere] + [vmem] * 5,
+        out_specs=(vmem, vmem, vmem, anywhere, anywhere, anywhere),
         scratch_shapes=[
             pltpu.VMEM((2, tall, width), BF16),
             pltpu.VMEM((2, tall, width), BF16),
@@ -334,6 +400,13 @@
             pltpu.VMEM((deep, hid), BF16),
             pltpu.VMEM((hid, deep), BF16),
             pltpu.VMEM((team * mixer_out.shape[0], mixer_out.shape[1]), BF16),
+            pltpu.VMEM((2, toks, width), BF16),
+            pltpu.VMEM((short, width), BF16),
+            pltpu.VMEM((short, width), BF16),
+            pltpu.VMEM((toks, width), BF16),
+            pltpu.VMEM((toks, width), BF16),
+            dma((3,)),
+            dma((3,)),
             dma((3,)),
             dma((3,)),
             dma((2, count)),
@@ -350,7 +423,7 @@
         compiler_params=pltpu.CompilerParams(
             collective_id=0, has_side_effects=True, vmem_limit_bytes=60 * 1024 * 1024
         ),
-    )(send_rows, send_cot, w_gate, w_up, w_down, mixer_out)
+    )(send_rows, send_cot, w_gate, w_up, w_down, mixer_out, stream, out_grad, pick, scale)
 
 
 def mixer_kernel(
@@ -584,23 +657,34 @@
     route_total = tok_rows * top_count
     slots = experts * capacity
     me = lax.axis_index("sp")
-    relative = lax.rem(route_ids - me + experts, experts)
-    flat = relative.reshape(route_total)
+    ring = experts // 2
+    away = (route_ids // ring != me // ring).astype(jnp.int32)
+    flat = (away * ring + lax.rem(route_ids - me + experts, ring)).reshape(route_total)
     one_hot = flat[:, None] == jnp.arange(experts, dtype=jnp.int32)[None, :]
     order = jnp.arange(route_total, dtype=jnp.int32)
     earlier = (order[:, None] > order[None, :]).astype(BF16)
     ranks = dot(earlier, one_hot.astype(BF16), 1, 0)
     slot_pos = jnp.sum(jnp.where(one_hot, ranks, 0.0), axis=1).astype(jnp.int32)
     slot_of = (flat * capacity + slot_pos).reshape(tok_rows, top_count)
-    places = jnp.arange(slots, dtype=jnp.int32)
-    hits = [slot_of[:, k][None, :] == places[:, None] for k in range(top_count)]
-    slot_weight = sum(
-        jnp.sum(jnp.where(hits[k], route_weights[:, k][None, :], 0.0), axis=1)
-        for k in range(top_count)
+    short = slots // 2
+    places = jnp.arange(short, dtype=jnp.int32)
+
+    def placed_by(slot_rows, weight_rows):
+        hits = [row[None, :] == places[:, None] for row in slot_rows]
+        weights = sum(
+            jnp.sum(jnp.where(hit, row[None, :], 0.0), axis=1)
+            for hit, row in zip(hits, weight_rows)
+        )
+        return functools.reduce(jnp.logical_or, hits).astype(BF16), weights[:, None]
+
+    table = jnp.concatenate([(slot_of - short).T.astype(F32), route_weights.T], axis=0)
+    across = lax.ppermute(table, "sp", [(i, (i + ring) % experts) for i in range(experts)])
+    pick_far, scale_far = placed_by(
+        across[:top_count].astype(jnp.int32), across[top_count:]
     )
-    pick = functools.reduce(jnp.logical_or, hits).astype(BF16)
+    pick, slot_weight = placed_by(slot_of.T, route_weights.T)
     send_rows = dot(pick, stream, 1, 0).astype(BF16)
-    send_cot = (slot_weight[:, None] * dot(pick, out_grad, 1, 0)).astype(BF16)
+    send_cot = (slot_weight * dot(pick, out_grad, 1, 0)).astype(BF16)
     depth = taps.shape[0]
     channels = conv_gate.shape[1]
     prod_rows = conv_gate.astype(jnp.float32) * conv_value.astype(jnp.float32)
@@ -610,10 +694,20 @@
     for tap_index in range(depth):
         conv_sum = conv_sum + taps[tap_index][None, :] * padded[tap_index : tap_index + tok_rows]
     mixer_out = (gate_in.astype(jnp.float32) * conv_sum).astype(jnp.bfloat16)
-    back, mix, gate_w_grad, up_w_grad, down_w_grad = expert_pass(
-        send_rows, send_cot, w_gate, w_up, w_down, mixer_out, capacity
+    back, crossed, mix, gate_w_grad, up_w_grad, down_w_grad = expert_pass(
+        send_rows,
+        send_cot,
+        w_gate,
+        w_up,
+        w_down,
+        mixer_out,
+        stream,
+        out_grad,
+        pick_far,
+        scale_far,
+        capacity,
     )
-    input_grad = dot(pick, back, 0, 0)
+    input_grad = dot(pick, back, 0, 0) + crossed.astype(F32)
     stream_half = (out_grad.astype(jnp.float32) + input_grad).astype(jnp.bfloat16)
     if w_out.shape[0] // lax.axis_size("sp") % 128 == 0:
         out_proj_grad, mixer_grad, halo = mixer_pass(stream_half, w_out, mix, gate_in)

time: 219 us -> 188 us (0.86)
  Pallas kernels: 186 us -> 151 us
  starting transfers between devices: 4.87 us -> 7.59 us
  local copies, waits for them, and re-layouts: 2.04 us -> 4.31 us
    pallas_call x1, Pallas kernels: 169 us -> 131 us  [expert_pass(): pl.pallas_call(functools.partial(expert_kernel, count, cap), out_shape=(j...]
    ppermute x0 -> x1, starting transfers between devices: none -> 4.06 us  [shards(): lax.ppermute(table, 'sp', [(i, (i + ring) % experts) for i in range(exper...]
    pallas_call x1, Pallas kernels: 16.9 us -> 20.6 us  [mixer_pass(): pl.pallas_call(functools.partial(mixer_kernel, count), out_shape=(jax.Sha...]
  transfers between devices with their start and end apart: 1 -> 2, of which waited for: 0 -> 0; matrix products, arithmetic and copies ran while one was open for 3% -> 4% of each run, Pallas kernels for 0% -> 0%
where the time goes in v3:
time: 188 us; the launch traced here: 185 us
  Pallas kernels  151 us (80%)
  other arithmetic  15.7 us (8%)
  starting transfers between devices  7.59 us (4%)
  matrix products  5.13 us (3%)
  local copies, waits for them, and re-layouts  4.31 us (2%)
    pallas_call x1, Pallas kernels, expert_pass(): pl.pallas_call(functools.partial(expert_kernel, count, cap), out_shape=(j...  131 us
    pallas_call x1, Pallas kernels, mixer_pass(): pl.pallas_call(functools.partial(mixer_kernel, count), out_shape=(jax.Sha...  20.6 us
    dot_general x4, matrix products, dot(): lax.dot_general(a, b, (((ca,), (cb,)), ((), ())), preferred_element_type=...  5.13 us
    ppermute x1, starting transfers between devices, shards(): lax.ppermute(table, 'sp', [(i, (i + ring) % experts) for i in range(exper...  4.06 us
  transfers between devices with their start and end apart: 2, of which 0 were waited for; matrix products, arithmetic and copies ran while one was open for 4% of the time, Pallas kernels for 0%

profile of v3, /device:TPU:0, one launch (start us, length us, event | category | flops | bytes accessed | tf_op | source)
XLA Modules:
  0.0 184.9 jit_solution(8953270812452747253)
XLA Ops:
  0.7 0.8 fusion.30
  1.7 0.3 fusion.2
  2.2 0.7 convert_bitcast_fusion
  3.0 0.7 pad_maximum_fusion.2
  3.7 4.1 %collective-permute-start.1 = (f32[4,256]{1,0:T(4,128)S(1)}, f32[4,256]{1,0:T(4,128)S(1)}, u32[]{:S(2)}, u32[]{:S(2)}) collective-permute-start(f32[4,256]{1,0:T(4,128)S(1)} %pad_maximum_fusion.2), channel_id=1, source_target_pairs={{0,16},{2,18},{4,20},{6,22},{8,24},{10,26},{12,28},{14,30},{16,0},... | collective-permute-start | bytes 12296 | tf_op jit(solution)/shard_map/ppermute | solution.py:681
  7.7 1.1 convert_multiply_fusion.3
  8.9 3.5 %collective-permute-start = (f32[2,512]{1,0:T(2,128)S(1)}, f32[2,512]{1,0:T(2,128)S(1)}, u32[]{:S(2)}, u32[]{:S(2)}) collective-permute-start(f32[2,512]{1,0:T(2,128)S(1)} %slice.46), channel_id=1, source_target_pairs={{0,2},{2,4},{4,6},{6,8},{8,10},{10,12},{12,14},{14,16},{16,18},{18... | collective-permute-start | bytes 12296 | tf_op jit(solution)/shard_map/ppermute | solution.py:19
  12.4 0.8 fusion.38
  13.2 1.4 convolution_convert_fusion.send_rows
  14.8 1.4 multiply_convert_fusion.send_cot
  16.3 0.8 fusion.19.pick
  17.3 0.9 copy.70.scale
  18.2 0.9 fusion.11
  19.1 130.7 %shard_map.179 = (bf16[512,1024]{1,0:T(8,128)(2,1)}, bf16[256,1024]{1,0:T(8,128)(2,1)}, bf16[1024,512]{1,0:T(8,128)(2,1)}, bf16[1,2048,512]{2,1,0:T(8,128)(2,1)}...) custom-call(bf16[512,1024]{1,0:T(8,128)(2,1)} %convolution_convert_fusion.send_rows, ...), custom_call_target="tpu_custom_call" | custom-call | tf_op jit(solution)/shard_map/pallas_call | solution.py:372
  149.8 2.0 %fusion.1.sh = bf16[256,1024]{1,0:T(8,128)(2,1)S(1)} fusion(bf16[512,1024]{1,0:T(8,128)(2,1)} %get-tuple-element.17, bf16[256,1024]{1,0:T(8,128)(2,1)} %get-tuple-element.18, bf16[256,1024]{1,0:T(8,128)(2,1)S(1)} %copy-done.11, s32[256]{0:T(256)S(1)} %bitcast.33, s32[256]{0:T(256)S(1)} %bitcast.29), kind=kOutput, calls=%fused_computation.4 | convolution fusion | flops 270139392 | bytes 2623488 | tf_op jit(solution)/shard_map/dot_general | solution.py:23
  151.9 1.4 copy-done.2
  153.3 20.6 %shard_map.180 = (f32[128,512]{1,0:T(8,128)S(1)}, bf16[256,512]{1,0:T(8,128)(2,1)S(1)}, f32[8,512]{1,0:T(8,128)S(1)}) custom-call(bf16[256,1024]{1,0:T(8,128)(2,1)S(1)} %fusion.1.sh, bf16[2048,512]{1,0:T(8,128)(2,1)S(1)} %copy-done.1, bf16[1024,512]{1,0:T(8,128)(2,1)S(1)} %copy-done.2, bf16[256,512]{1,0:T(8,128)(2,1)S(1)} %copy-done), custom_call_target="tpu_custom_call" | custom-call | tf_op jit(solution)/shard_map/pallas_call | solution.py:605
  173.9 0.8 convert_multiply_fusion
  174.7 0.9 fusion.12
  175.6 0.8 fusion.13
  176.4 2.6 %convert_element_type.93 = f32[1,2048,512]{2,1,0:T(8,128)} convert(bf16[1,2048,512]{2,1,0:T(8,128)(2,1)S(1)} %copy-done.6) | non-fusion elementwise | flops 1048576 | bytes 6291456 | tf_op jit(solution)/shard_map/convert_element_type | solution.py:739
  179.0 2.6 %convert_element_type.94 = f32[1,2048,512]{2,1,0:T(8,128)} convert(bf16[1,2048,512]{2,1,0:T(8,128)(2,1)S(1)} %copy-done.5) | non-fusion elementwise | flops 1048576 | bytes 6291456 | tf_op jit(solution)/shard_map/convert_element_type | solution.py:740
  181.6 2.5 %convert_element_type.95 = f32[1,512,2048]{2,1,0:T(8,128)} convert(bf16[1,512,2048]{2,1,0:T(8,128)(2,1)S(1)} %copy-done.4) | non-fusion elementwise | flops 1048576 | bytes 6291456 | tf_op jit(solution)/shard_map/convert_element_type | solution.py:741
  184.2 0.7 copy.72
  (43 shorter events, 1.1 us)
Async XLA Ops:
  0.6 12.5 %copy-start.7 = (bf16[256,1024]{1,0:T(8,128)(2,1)S(1)}, bf16[256,1024]{1,0:T(8,128)(2,1)}, u32[]{:S(2)}) copy-start(bf16[256,1024]{1,0:T(8,128)(2,1)} %stream_in.1) | copy-start | bytes 1572868
  0.6 14.2 %copy-start.10 = (bf16[256,1024]{1,0:T(8,128)(2,1)S(1)}, bf16[256,1024]{1,0:T(8,128)(2,1)}, u32[]{:S(2)}) copy-start(bf16[256,1024]{1,0:T(8,128)(2,1)} %grad_in.1) | copy-start | bytes 1572868
  3.7 12.6 %copy-start.12 = (f32[3,512]{1,0:T(4,128)S(1)}, f32[3,512]{1,0:T(4,128)}, u32[]{:S(2)}) copy-start(f32[3,512]{1,0:T(4,128)} %param.17) | copy-start | bytes 18436
  3.7 12.6 %collective-permute-start.1 = (f32[4,256]{1,0:T(4,128)S(1)}, f32[4,256]{1,0:T(4,128)S(1)}, u32[]{:S(2)}, u32[]{:S(2)}) collective-permute-start(f32[4,256]{1,0:T(4,128)S(1)} %pad_maximum_fusion.2), channel_id=1, source_target_pairs={{0,16},{2,18},{4,20},{6,22},{8,24},{10,26},{12,28},{14,30},{16,0},... | collective-permute-start | bytes 12296 | tf_op jit(solution)/shard_map/ppermute | solution.py:681
  8.8 9.4 %copy-start = (bf16[256,512]{1,0:T(8,128)(2,1)S(1)}, bf16[256,512]{1,0:T(8,128)(2,1)}, u32[]{:S(2)}) copy-start(bf16[256,512]{1,0:T(8,128)(2,1)} %gate_in.1) | copy-start | bytes 786436
  8.9 9.4 %collective-permute-start = (f32[2,512]{1,0:T(2,128)S(1)}, f32[2,512]{1,0:T(2,128)S(1)}, u32[]{:S(2)}, u32[]{:S(2)}) collective-permute-start(f32[2,512]{1,0:T(2,128)S(1)} %slice.46), channel_id=1, source_target_pairs={{0,2},{2,4},{4,6},{6,8},{8,10},{10,12},{12,14},{14,16},{16,18},{18... | collective-permute-start | bytes 12296 | tf_op jit(solution)/shard_map/ppermute | solution.py:19
  19.1 130.7 %copy-start.11 = (bf16[256,1024]{1,0:T(8,128)(2,1)S(1)}, bf16[256,1024]{1,0:T(8,128)(2,1)}, u32[]{:S(2)}) copy-start(bf16[256,1024]{1,0:T(8,128)(2,1)} %grad_in.1) | copy-start | bytes 1572868
  149.8 2.1 %copy-start.1 = (bf16[2048,512]{1,0:T(8,128)(2,1)S(1)}, bf16[2048,512]{1,0:T(8,128)(2,1)}, u32[]{:S(2)}) copy-start(bf16[2048,512]{1,0:T(8,128)(2,1)} %w_out_hbm.1) | copy-start | bytes 6291460
  151.8 22.9 %copy-start.3 = (bf16[256,1024]{1,0:T(8,128)(2,1)}, bf16[256,1024]{1,0:T(8,128)(2,1)S(1)}, u32[]{:S(2)}) copy-start(bf16[256,1024]{1,0:T(8,128)(2,1)S(1)} %fusion.1.sh) | copy-start | bytes 1572868
  151.9 1.4 copy-start.2
  153.3 21.4 %copy-start.8 = (bf16[256,512]{1,0:T(8,128)(2,1)S(1)}, bf16[256,512]{1,0:T(8,128)(2,1)}, u32[]{:S(2)}) copy-start(bf16[256,512]{1,0:T(8,128)(2,1)} %param.15) | copy-start | bytes 786436
  173.9 1.8 copy-start.9
  173.9 2.5 %copy-start.6 = (bf16[1,2048,512]{2,1,0:T(8,128)(2,1)S(1)}, bf16[1,2048,512]{2,1,0:T(8,128)(2,1)}, u32[]{:S(2)}) copy-start(bf16[1,2048,512]{2,1,0:T(8,128)(2,1)} %get-tuple-element.23) | copy-start | bytes 6291460
  176.4 2.6 %copy-start.5 = (bf16[1,2048,512]{2,1,0:T(8,128)(2,1)S(1)}, bf16[1,2048,512]{2,1,0:T(8,128)(2,1)}, u32[]{:S(2)}) copy-start(bf16[1,2048,512]{2,1,0:T(8,128)(2,1)} %get-tuple-element.24) | copy-start | bytes 6291460
  179.0 2.6 %copy-start.4 = (bf16[1,512,2048]{2,1,0:T(8,128)(2,1)S(1)}, bf16[1,512,2048]{2,1,0:T(8,128)(2,1)}, u32[]{:S(2)}) copy-start(bf16[1,512,2048]{2,1,0:T(8,128)(2,1)} %get-tuple-element.25) | copy-start | bytes 6291460
